TPU v7x, 512 devices: a whole 4x8x8 slice. The times are simulated.
512 devices in a mesh: sp: 64 (over z, y), dp: 8 (over x, core).
Axes of the slice: x: 4, y: 8, z: 8, core: 2. Of those that a mesh axis runs over, the one named last changes fastest.
Arguments:
- glu_value: bfloat16 [8, 32768, 512], P('dp', 'sp'), may hold values from -6 to 6
- glu_gate: bfloat16 [8, 32768, 512], P('dp', 'sp'), may hold values from -8 to 8
- cotangent: bfloat16 [8, 32768, 2048], P('dp', 'sp'), may hold values from -8 to 8
- conv_weight: float32 [31, 512], replicated, may hold values from -1 to 1
- norm_gain: float32 [512], replicated, may hold values from 0.1 to 1.9
- norm_shift: float32 [512], replicated, may hold values from -3 to 3
- out_weight: bfloat16 [2048, 512], P('dp'), may hold values from -0.25 to 0.25
Outputs:
- grad_value: bfloat16 [8, 32768, 512], P('dp', 'sp')
- grad_gate: bfloat16 [8, 32768, 512], P('dp', 'sp')
- grad_out_weight: float32 [2048, 512], P('dp')
- grad_conv: float32 [31, 512], replicated
- grad_gain: float32 [512], replicated
- grad_shift: float32 [512], replicated
All inputs are finite; a program needn't handle non-finite values.
Results may differ from a plain program's by a relative error of at most 0.003.
Values may be sent and summed in bfloat16 or wider, within the bound.
No kernel may reach another device: no remote copies, remote signals or barrier semaphores. Data moves between devices by JAX's collectives and lax.ppermute only.
A program may use at most 64 MiB of HBM per device.

v0:
```python
import functools
import math

import jax
import jax.numpy as jnp
from jax import lax
from jax.sharding import Mesh
from jax.sharding import PartitionSpec as P

SP = ("sp_0", "sp_1")
DP = ("dp_0", "dp_1")
SP_DP = ("sp_0", "sp_1", "dp_0", "dp_1")


epsilon = 1e-06


def from_behind(value, axis, by):
    count = lax.axis_size(axis)
    pairs = [(i, i + by) for i in range(count) if 0 <= i + by < count]
    return lax.ppermute(value, axis, pairs)


def from_everyone(value, axis):
    count = lax.axis_size(axis)
    return lax.all_to_all(
        jnp.broadcast_to(value[None], (count, *value.shape)), axis, 0, 0, tiled=True
    )


def joined_along(pieces, dim):
    pieces = jnp.moveaxis(pieces, 0, dim)
    dims = pieces.shape
    return pieces.reshape(*dims[:dim], dims[dim] * dims[dim + 1], *dims[dim + 2 :])


def whole_of(value, axes, dim):
    far, near = axes
    initial = from_everyone(value, far)
    pieces = jnp.swapaxes(from_everyone(initial, near), 0, 1)
    return joined_along(pieces.reshape(-1, *value.shape), dim)


def over_axes(value, axes):
    return functools.reduce(lax.psum, axes, value)


def cut_along(value, dim, count):
    before, after = (value.shape[:dim], value.shape[dim + 1 :])
    return jnp.moveaxis(value.reshape(*before, count, -1, *after), dim, 0)


def sent_and_summed(value, axis, dim):
    pieces = cut_along(value, dim, lax.axis_size(axis))
    arrived = lax.all_to_all(pieces, axis, split_axis=0, concat_axis=0, tiled=True)
    return arrived.sum(axis=0)


def sum_in_two_steps(value, axes, dim):
    far, near = axes
    own = sent_and_summed(cut_along(value, dim, lax.axis_size(far)), near, dim + 1)
    return jnp.sum(lax.all_to_all(own, far, 0, 0, tiled=True), axis=0)


def rows_for(lines, count):
    spare = -len(lines) % count
    return jnp.pad(lines, [(0, spare)] + [(0, 0)] * (lines.ndim - 1))


def gathered_copies(value, axis, dim):
    return joined_along(from_everyone(value, axis), dim)


def nested_sum(value, axes):
    lines = value.reshape(-1, value.shape[-1])
    padded = rows_for(lines, lax.axis_size(axes))
    whole = gathered_copies(sent_and_summed(padded, axes, 0), axes, 0)
    return lax.slice_in_dim(whole, 0, len(lines)).reshape(value.shape)


def per_device(glu_value, glu_gate, cotangent, conv_weight, norm_gain, norm_shift, out_weight):
    value_rows = glu_value[0]
    gate_rows = glu_gate[0]
    cotan_rows = cotangent[0]
    length = value_rows.shape[0]
    channels = value_rows.shape[1]
    tap_count = conv_weight.shape[0]
    halo_rows = tap_count - 1
    count_sp = lax.axis_size(SP)
    count_dp = lax.axis_size(DP)
    scale = 1.0 / math.sqrt(length * count_sp * count_dp)
    prior_value, prior_gate = from_behind(
        (value_rows[length - halo_rows :], gate_rows[length - halo_rows :]), SP, 1
    )
    value_ext = jnp.concatenate([prior_value, value_rows], axis=0).astype(jnp.float32)
    gate_ext = jnp.concatenate([prior_gate, gate_rows], axis=0).astype(jnp.float32)
    gated_ext = value_ext * jax.nn.sigmoid(gate_ext)
    conv_rows = jnp.zeros((length, channels), jnp.float32)
    for offset in range(tap_count):
        conv_rows = conv_rows + conv_weight[offset] * gated_ext[offset : offset + length]
    centred = conv_rows - jnp.mean(conv_rows, axis=-1, keepdims=True)
    inv_std = lax.rsqrt(jnp.mean(centred * centred, axis=-1, keepdims=True) + epsilon)
    normed = centred * inv_std
    pre_act = normed * norm_gain + norm_shift
    sigmoid_pre = jax.nn.sigmoid(pre_act)
    act_rows = (pre_act * sigmoid_pre).astype(jnp.bfloat16)
    columns = cotan_rows
    grad_act = jnp.dot(
        columns, whole_of(out_weight, ("dp_0", "dp_1"), 0), preferred_element_type=jnp.float32
    )
    grad_pre = grad_act * sigmoid_pre * (1.0 + pre_act * (1.0 - sigmoid_pre))
    grad_normed = grad_pre * norm_gain
    grad_conv_rows = inv_std * (
        grad_normed
        - jnp.mean(grad_normed, axis=-1, keepdims=True)
        - normed * jnp.mean(grad_normed * normed, axis=-1, keepdims=True)
    )
    later_grads = from_behind(grad_conv_rows[:halo_rows], SP, -1)
    padded_grad = jnp.concatenate([grad_conv_rows, later_grads], axis=0)
    grad_gated = jnp.zeros((length, channels), jnp.float32)
    for offset in range(tap_count):
        start = tap_count - 1 - offset
        grad_gated = grad_gated + conv_weight[offset] * padded_grad[start : start + length]
    grad_taps = jnp.stack(
        [
            jnp.sum(grad_conv_rows * gated_ext[offset : offset + length], axis=0)
            for offset in range(tap_count)
        ],
        axis=0,
    )
    sigmoid_gate = jax.nn.sigmoid(gate_ext[halo_rows:])
    grad_value = (grad_gated * sigmoid_gate).astype(jnp.bfloat16)
    grad_gate = (grad_gated * value_ext[halo_rows:] * sigmoid_gate * (1.0 - sigmoid_gate)).astype(
        jnp.bfloat16
    )
    grad_conv, grad_gain, grad_shift = (
        over_axes(grad_taps * scale, SP_DP),
        over_axes(jnp.sum(grad_pre * normed, axis=0) * scale, SP_DP),
        over_axes(jnp.sum(grad_pre, axis=0) * scale, SP_DP),
    )
    columns = cotan_rows
    product = lax.dot_general(
        columns, act_rows, (((0,), (0,)), ((), ())), preferred_element_type=jnp.float32
    )
    partial_rows = sum_in_two_steps(product * scale, ("dp_0", "dp_1"), 0)
    grad_out_weight = nested_sum(partial_rows, SP)
    return (grad_value[None], grad_gate[None], grad_out_weight, grad_conv, grad_gain, grad_shift)


def solution(mesh):
    split = Mesh(mesh.devices.reshape(8, 8, 4, 2), ("sp_0", "sp_1", "dp_0", "dp_1"))
    return jax.shard_map(
        per_device,
        mesh=split,
        in_specs=(P(DP, SP, None), P(DP, SP, None), P(DP, SP, None), P(), P(), P(), P(DP, None)),
        out_specs=(P(DP, SP, None), P(DP, SP, None), P(DP, None), P(), P(), P()),
        check_vma=False,
    )
```

profile of v0, /device:TPU:1, one launch (start us, length us, event | category | flops | bytes accessed | tf_op | source)
XLA Modules:
  0.0 391.4 jit_solution(5961407943740370128)
XLA Ops:
  7.2 0.9 slice_bitcast_fusion
  8.1 4.0 %collective-permute-start.1 = (bf16[30,512]{1,0:T(8,128)(2,1)S(1)}, bf16[30,512]{1,0:T(8,128)(2,1)S(1)}, u32[]{:S(2)}, u32[]{:S(2)}) collective-permute-start(bf16[30,512]{1,0:T(8,128)(2,1)S(1)} %slice_bitcast_fusion), channel_id=1, source_target_pairs={{0,8},{8,16},{16,24},{24,32},{32,40},{40,48},{48,56},{56,64},{64,7... | collective-permute-start | bytes 92168 | tf_op jit(solution)/shard_map/ppermute | solution.py:21
  12.1 0.8 slice_bitcast_fusion.1
  12.9 3.2 collective-permute-start
  16.1 1.1 fusion.114
  17.2 1.1 fusion.115
  18.3 1.6 divide_multiply_fusion
  20.0 5.0 %fusion.113 = (f32[512]{0:T(512)S(1)}, f32[512,512]{1,0:T(8,128)S(1)}) fusion(f32[542,512]{1,0:T(8,128)S(1)} %divide_multiply_fusion, f32[512]{0:T(512)S(1)} %bitcast.158, f32[512]{0:T(512)S(1)} %bitcast.160, f32[512]{0:T(512)S(1)} %bitcast.102, f32[512]{0:T(512)S(1)} %bitcast.104, f32[512]{0:T(512)S(1)} %bitcast.106, f32[512]{0:T(512)S(1)} %bitcast.108, ...), kind=kLoop, calls=%fused_computation.213 | loop fusion | flops 16252416 | bytes 33619968 | tf_op jit(solution)/shard_map/reduce_sum | solution.py:101
  25.2 0.8 copy-done.2
  26.0 3.4 multiply_bitcast_fusion
  29.4 6.6 %reshape_reshape.7 = f32[4,2,256,512]{2,1,0,3:T(2,128)} reshape(f32[2048,512]{0,1:T(8,128)} %multiply_bitcast_fusion) | data formatting | bytes 8388608 | tf_op jit(solution)/shard_map/reshape;reshape | solution.py:50
  36.0 3.3 copy.30
  39.3 10.1 %all_to_all.30 = f32[2,4,256,512]{2,1,3,0:T(4,128)} all-to-all(f32[2,4,256,512]{2,1,3,0:T(4,128)S(1)} %bitcast.94), channel_id=1, replica_groups=mesh['sp_0'=8,'sp_1'=8,'dp_0'=4,'dp_1'=2] {'dp_1'}, dimensions={0} | all-to-all | bytes 8388608 | tf_op jit(solution)/shard_map/all_to_all | solution.py:55
  49.4 1.1 broadcast_in_dim.10
  50.5 4.2 %all-to-all-start = ((bf16[4,256,512]{2,1,0:T(8,128)(2,1)}), bf16[4,256,512]{2,1,0:T(8,128)(2,1)}, u32[]{:S(2)}, u32[]{:S(2)}) async-start(bf16[4,256,512]{2,1,0:T(8,128)(2,1)} %broadcast_in_dim.10), calls=%async_computation | async-start | bytes 2097152 | tf_op jit(solution)/shard_map/all_to_all | solution.py:26
  54.7 5.1 %reduce_sum.364 = f32[4,256,512]{1,0,2:T(4,128)} reduce(f32[2,4,256,512]{2,1,3,0:T(4,128)} %all_to_all.30, f32[]{:T(128)} %constant.5.clone.1), dimensions={0}, to_apply=%region_4.0 | reduce | flops 524288 | bytes 6291460 | tf_op jit(solution)/shard_map/reduce_sum | solution.py:56
  59.8 3.3 copy.24
  63.1 6.5 %all-to-all-done = bf16[4,256,512]{2,1,0:T(8,128)(2,1)} async-done(((bf16[4,256,512]{2,1,0:T(8,128)(2,1)}), bf16[4,256,512]{2,1,0:T(8,128)(2,1)}, u32[]{:S(2)}, u32[]{:S(2)}) %all-to-all-start) | async-done | bytes 1048608 | tf_op jit(solution)/shard_map/all_to_all | solution.py:26
  69.6 1.4 broadcast_in_dim.11
  71.0 7.2 %all_to_all.31 = bf16[2,4,256,512]{3,2,1,0:T(8,128)(2,1)} all-to-all(bf16[2,4,256,512]{3,2,1,0:T(8,128)(2,1)S(1)} %broadcast_in_dim.11), channel_id=1, replica_groups=mesh['sp_0'=8,'sp_1'=8,'dp_0'=4,'dp_1'=2] {'dp_1'}, dimensions={0} | all-to-all | bytes 4194304 | tf_op jit(solution)/shard_map/all_to_all | solution.py:26
  78.2 4.6 %all-to-all-start.3 = ((f32[4,256,512]{1,2,0:T(8,128)}), f32[4,256,512]{1,2,0:T(8,128)}, u32[]{:S(2)}, u32[]{:S(2)}) async-start(f32[4,256,512]{1,2,0:T(8,128)} %copy.24), calls=%async_computation.3 | async-start | bytes 4194304 | tf_op jit(solution)/shard_map/all_to_all | solution.py:62
  82.8 1.9 copy.21
  84.7 1.8 multiply_reduce_fusion
  86.6 3.9 %multiply_reduce_fusion.1 = (f32[512]{0:T(512)S(1)}, f32[512]{0:T(512)S(1)}, f32[512]{0:T(512)S(1)}, f32[512]{0:T(512)S(1)}, f32[512]{0:T(512)S(1)}, /*index=5*/...) fusion(f32[542,512]{1,0:T(8,128)S(1)} %divide_multiply_fusion, ...), kind=kLoop, calls=%fused_computation.153 | loop fusion | flops 11262976 | bytes 22067200 | tf_op jit(solution)/shard_map/reduce_sum | solution.py:126
  90.5 18.2 %all-to-all-done.3 = f32[4,256,512]{1,2,0:T(8,128)} async-done(((f32[4,256,512]{1,2,0:T(8,128)}), f32[4,256,512]{1,2,0:T(8,128)}, u32[]{:S(2)}, u32[]{:S(2)}) %all-to-all-start.3) | async-done | bytes 2097184 | tf_op jit(solution)/shard_map/all_to_all | solution.py:62
  108.8 2.6 reduce_sum.365
  111.3 2.0 copy.26
  113.4 2.0 reshape.45
  115.3 16.0 %all-to-all-start.4 = ((f32[64,4,512]{2,1,0:T(4,128)}), f32[64,4,512]{2,1,0:T(4,128)}, u32[]{:S(2)}, u32[]{:S(2)}) async-start(f32[64,4,512]{2,1,0:T(4,128)} %reshape.45), calls=%async_computation.4 | async-start | bytes 1048576 | tf_op jit(solution)/shard_map/all_to_all | solution.py:55
  131.4 2.7 multiply_reduce_fusion.19
  134.3 0.6 broadcast_multiply_fusion.1
  134.9 0.6 broadcast_multiply_fusion
  135.6 2.2 maximum_convert_fusion.1
  137.9 1.3 collective-permute-start.2
  139.2 67.9 %all-reduce.11.cloned.1.call-done = (f32[31,512]{1,0:T(8,128)}, f32[512]{0:T(512)}, f32[512]{0:T(512)}) async-done(((f32[31,512]{1,0:T(8,128)}, f32[512]{0:T(512)}, f32[512]{0:T(512)}), (f32[31,512]{1,0:T(8,128)}, f32[512]{0:T(512)}, f32[512]{0:T(512)})) %all-reduce.11.cloned.1.call-update) | async-done | bytes 67600 | tf_op jit(solution)/shard_map/psum | solution.py:45
  207.2 2.3 maximum_convert_fusion
  209.4 74.0 %all-reduce.9.cloned.1.call-done = (f32[31,512]{1,0:T(8,128)}, f32[512]{0:T(512)}, f32[512]{0:T(512)}) async-done(((f32[31,512]{1,0:T(8,128)}, f32[512]{0:T(512)}, f32[512]{0:T(512)}), (f32[31,512]{1,0:T(8,128)}, f32[512]{0:T(512)}, f32[512]{0:T(512)})) %all-reduce.9.cloned.1.call-update) | async-done | bytes 67600 | tf_op jit(solution)/shard_map/psum | solution.py:45
  283.5 1.2 reduce_sum.366
  284.6 0.9 broadcast_in_dim.14
  285.5 11.3 %all-to-all-start.5 = ((f32[64,4,512]{2,1,0:T(4,128)}), f32[64,4,512]{2,1,0:T(4,128)}, u32[]{:S(2)}, u32[]{:S(2)}) async-start(f32[64,4,512]{2,1,0:T(4,128)} %broadcast_in_dim.14), calls=%async_computation.5 | async-start | bytes 1048576 | tf_op jit(solution)/shard_map/all_to_all | solution.py:26
  296.8 7.3 %fusion.105 = (bf16[1,512,512]{2,1,0:T(8,128)(2,1)}, f32[512,512]{1,0:T(8,128)}) fusion(f32[542,512]{1,0:T(8,128)} %maximum_convert_fusion, f32[542,512]{1,0:T(8,128)} %maximum_convert_fusion.1, f32[512,512]{1,0:T(8,128)S(1)} %copy-done.1, f32[512]{0:T(512)S(1)} %bitcast.159, f32[30,512]{1,0:T(8,128)S(1)} %collective-permute-done.2, f32[512]{0:T(512)S(1)} %bitcast.161, ...), kind=kLoop, calls=%fused_computation.197 | loop fusion | flops 25952256 | bytes 4843520 | tf_op jit(solution)/shard_map/broadcast_in_dim | solution.py:147
  304.1 35.2 %all-reduce.13.cloned.1.call-done = (f32[31,512]{1,0:T(8,128)}, f32[512]{0:T(512)}, f32[512]{0:T(512)}) async-done(((f32[31,512]{1,0:T(8,128)}, f32[512]{0:T(512)}, f32[512]{0:T(512)}), (f32[31,512]{1,0:T(8,128)}, f32[512]{0:T(512)}, f32[512]{0:T(512)})) %all-reduce.13.cloned.1.call-update) | async-done | bytes 67600 | tf_op jit(solution)/shard_map/psum | solution.py:45
  339.3 2.6 fusion.104
  341.9 2.0 reshape.46
  344.0 36.9 %all-reduce.15.cloned.1.call-done = (f32[31,512]{1,0:T(8,128)}, f32[512]{0:T(512)}, f32[512]{0:T(512)}) async-done(((f32[31,512]{1,0:T(8,128)}, f32[512]{0:T(512)}, f32[512]{0:T(512)}), (f32[31,512]{1,0:T(8,128)}, f32[512]{0:T(512)}, f32[512]{0:T(512)})) %all-reduce.15.cloned.1.call-update) | async-done | bytes 67600 | tf_op jit(solution)/shard_map/psum | solution.py:45
  380.9 1.5 copy.43
  382.4 1.2 copy.44
  383.6 1.2 copy.45
  (32 shorter events, 0.7 us)
Async XLA Ops:
  7.2 18.9 %copy-start = (bf16[1,512,2048]{2,1,0:T(8,128)(2,1)S(1)}, bf16[1,512,2048]{2,1,0:T(8,128)(2,1)}, u32[]{:S(2)}) copy-start(bf16[1,512,2048]{2,1,0:T(8,128)(2,1)} %param.9) | copy-start | bytes 6291460
  8.1 10.2 %collective-permute-start.1 = (bf16[30,512]{1,0:T(8,128)(2,1)S(1)}, bf16[30,512]{1,0:T(8,128)(2,1)S(1)}, u32[]{:S(2)}, u32[]{:S(2)}) collective-permute-start(bf16[30,512]{1,0:T(8,128)(2,1)S(1)} %slice_bitcast_fusion), channel_id=1, source_target_pairs={{0,8},{8,16},{16,24},{24,32},{32,40},{40,48},{48,56},{56,64},{64,7... | collective-permute-start | bytes 92168 | tf_op jit(solution)/shard_map/ppermute | solution.py:21
  12.9 5.4 %collective-permute-start = (bf16[30,512]{1,0:T(8,128)(2,1)S(1)}, bf16[30,512]{1,0:T(8,128)(2,1)S(1)}, u32[]{:S(2)}, u32[]{:S(2)}) collective-permute-start(bf16[30,512]{1,0:T(8,128)(2,1)S(1)} %slice_bitcast_fusion.1), channel_id=1, source_target_pairs={{0,8},{8,16},{16,24},{24,32},{32,40},{40,48},{48,56},{56,64},{64,7... | collective-permute-start | bytes 92168 | tf_op jit(solution)/shard_map/ppermute | solution.py:21
  19.9 6.1 %copy-start.5 = (f32[512]{0:T(512)S(1)}, f32[512]{0:T(512)}, u32[]{:S(2)}) copy-start(f32[512]{0:T(512)} %param.11) | copy-start | bytes 6148
  19.9 6.1 %copy-start.6 = (f32[512]{0:T(512)S(1)}, f32[512]{0:T(512)}, u32[]{:S(2)}) copy-start(f32[512]{0:T(512)} %param.12) | copy-start | bytes 6148
  24.9 1.1 copy-start.2
  39.3 10.1 %copy-start.4 = (bf16[256,512]{1,0:T(8,128)(2,1)S(1)}, bf16[256,512]{1,0:T(8,128)(2,1)}, u32[]{:S(2)}) copy-start(bf16[256,512]{1,0:T(8,128)(2,1)} %param.13) | copy-start | bytes 786436
  50.5 19.1 %all-to-all-start = ((bf16[4,256,512]{2,1,0:T(8,128)(2,1)}), bf16[4,256,512]{2,1,0:T(8,128)(2,1)}, u32[]{:S(2)}, u32[]{:S(2)}) async-start(bf16[4,256,512]{2,1,0:T(8,128)(2,1)} %broadcast_in_dim.10), calls=%async_computation | async-start | bytes 2097152 | tf_op jit(solution)/shard_map/all_to_all | solution.py:26
  78.2 30.6 %all-to-all-start.3 = ((f32[4,256,512]{1,2,0:T(8,128)}), f32[4,256,512]{1,2,0:T(8,128)}, u32[]{:S(2)}, u32[]{:S(2)}) async-start(f32[4,256,512]{1,2,0:T(8,128)} %copy.24), calls=%async_computation.3 | async-start | bytes 4194304 | tf_op jit(solution)/shard_map/all_to_all | solution.py:62
  82.8 1.9 copy-start.3
  115.3 168.1 %all-to-all-start.4 = ((f32[64,4,512]{2,1,0:T(4,128)}), f32[64,4,512]{2,1,0:T(4,128)}, u32[]{:S(2)}, u32[]{:S(2)}) async-start(f32[64,4,512]{2,1,0:T(4,128)} %reshape.45), calls=%async_computation.4 | async-start | bytes 1048576 | tf_op jit(solution)/shard_map/all_to_all | solution.py:55
  131.4 75.7 %all-reduce.11.cloned.1.call-start = ((), (), s32[]{:S(2)}) async-start(), calls=%async_computation.7 | async-start | bytes 139264 | tf_op jit(solution)/shard_map/psum | solution.py:45
  134.2 3.7 copy-start.1
  135.6 147.8 %all-reduce.9.cloned.1.call-start = ((), (), s32[]{:S(2)}) async-start(), calls=%async_computation.6 | async-start | bytes 139264 | tf_op jit(solution)/shard_map/psum | solution.py:45
  137.9 159.0 %collective-permute-start.2 = (f32[30,512]{1,0:T(8,128)S(1)}, f32[30,512]{1,0:T(8,128)S(1)}, u32[]{:S(2)}, u32[]{:S(2)}) collective-permute-start(f32[30,512]{1,0:T(8,128)S(1)} %slice.489), channel_id=1, source_target_pairs={{8,0},{16,8},{24,16},{32,24},{40,32},{48,40},{56,48},{64,56},{72,6... | collective-permute-start | bytes 184328 | tf_op jit(solution)/shard_map/ppermute | solution.py:21
  207.1 132.2 %all-reduce.13.cloned.1.call-start = ((), (), s32[]{:S(2)}) async-start(), calls=%async_computation.8 | async-start | bytes 139264 | tf_op jit(solution)/shard_map/psum | solution.py:45
  285.5 56.5 %all-to-all-start.5 = ((f32[64,4,512]{2,1,0:T(4,128)}), f32[64,4,512]{2,1,0:T(4,128)}, u32[]{:S(2)}, u32[]{:S(2)}) async-start(f32[64,4,512]{2,1,0:T(4,128)} %broadcast_in_dim.14), calls=%async_computation.5 | async-start | bytes 1048576 | tf_op jit(solution)/shard_map/all_to_all | solution.py:26
  296.8 84.1 %all-reduce.15.cloned.1.call-start = ((), (), s32[]{:S(2)}) async-start(), calls=%async_computation.9 | async-start | bytes 139264 | tf_op jit(solution)/shard_map/psum | solution.py:45
Sparse Core Ops, SparseCore 0:
  135.7 71.3 all-reduce.10
  209.6 73.7 all-reduce.8
  285.9 53.3 all-reduce.12
  342.1 38.6 all-reduce.14
where the time goes:
time: 393 us; the launch traced here: 391 us
  waiting for transfers between devices  239 us (61%)
  starting transfers between devices  44.9 us (11%)
  other arithmetic  37.9 us (10%)
  local copies, waits for them, and re-layouts  33.2 us (8%)
  blocking collectives  17.3 us (4%)
  between operations  14 us (4%)
  matrix products  5.23 us (1%)
    psum x4, waiting for transfers between devices, over_axes(): return functools.reduce(lax.psum, axes, value)  214 us
    all_to_all x1, waiting for transfers between devices, sum_in_two_steps(): return jnp.sum(lax.all_to_all(own, far, 0, 0, tiled=True), axis=0)  18.2 us
    all_to_all x1, starting transfers between devices, sent_and_summed(): lax.all_to_all(pieces, axis, split_axis=0, concat_axis=0, tiled=True)  16 us
    all_to_all x2, starting transfers between devices, from_everyone(): lax.all_to_all(jnp.broadcast_to(value[None], (count, *value.shape)), axis...  15.5 us
    all_to_all x1, blocking collectives, sent_and_summed(): lax.all_to_all(pieces, axis, split_axis=0, concat_axis=0, tiled=True)  10.1 us
    another operation x2, local copies, waits for them, and re-layouts, cut_along(): return jnp.moveaxis(value.reshape(*before, count, -1, *after), dim, 0)  9.84 us
    ppermute x3, starting transfers between devices, from_behind(): return lax.ppermute(value, axis, pairs)  8.52 us
  transfers between devices with their start and end apart: 11, of which 6 were waited for; matrix products, arithmetic and copies ran while one was open for 11% of the time, Pallas kernels for 0%

commit v1 on v0

v1 whole, which is shorter than its diff:
```python
import functools
import math

import jax
import jax.numpy as jnp
from jax import lax
from jax.experimental import pallas as pl
from jax.experimental.pallas import tpu as pltpu
from jax.sharding import Mesh
from jax.sharding import PartitionSpec as P

SP = ("sp_0", "sp_1")
DP = ("dp_0", "dp_1")

epsilon = 1e-06

LANES = 128
HALO = 32
BF16 = jnp.bfloat16
F32 = jnp.float32
VMEM = pl.BlockSpec(memory_space=pltpu.VMEM)
SMEM = pl.BlockSpec(memory_space=pltpu.SMEM)
HBM = pl.BlockSpec(memory_space=pltpu.HBM)


def params(mib=16):
    return pltpu.CompilerParams(vmem_limit_bytes=mib * 1024 * 1024)


def cost(us):
    return pl.CostEstimate(flops=int(us * 5.0e8), bytes_accessed=1 << 20, transcendentals=0)


def sigmoid(x):
    return 0.5 * jnp.tanh(0.5 * x) + 0.5


def forward_kernel(
    taps_ref, gain_ref, shift_ref, halo_hbm, value_hbm, gate_hbm,
    act_hbm, normed_hbm, inv_hbm, slope_hbm, gated_hbm,
    halo_ref, value_ref, gate_ref, act_ref, normed_ref, inv_ref, slope_ref, gated_ref,
    in_sems, out_sems,
):
    length, channels = value_ref.shape
    blocks = channels // LANES
    tap_count = taps_ref.shape[0]
    loads = [
        pltpu.make_async_copy(halo_hbm, halo_ref, in_sems.at[0]),
        pltpu.make_async_copy(value_hbm, value_ref, in_sems.at[1]),
        pltpu.make_async_copy(gate_hbm, gate_ref, in_sems.at[2]),
    ]
    for load in loads:
        load.start()
    for load in loads:
        load.wait()
    for b in range(blocks):
        lanes = slice(b * LANES, (b + 1) * LANES)
        gated_ref[b, 0:HALO, :] = halo_ref[0:HALO, lanes].astype(F32) * sigmoid(
            halo_ref[HALO : 2 * HALO, lanes].astype(F32)
        )

        def gating(i, carry, b=b, lanes=lanes):
            rows = pl.ds(pl.multiple_of(i * 64, 64), 64)
            gated_ref[b, pl.ds(pl.multiple_of(HALO + i * 64, 32), 64), :] = value_ref[
                rows, lanes
            ].astype(F32) * sigmoid(gate_ref[rows, lanes].astype(F32))
            return carry

        lax.fori_loop(0, length // 64, gating, 0)

        def conv(i, carry, b=b, lanes=lanes):
            start = pl.multiple_of(i * 64, 64)
            total = jnp.zeros((64, LANES), F32)
            for j in range(tap_count):
                total = total + taps_ref[j : j + 1, lanes] * gated_ref[
                    b, pl.ds(start + (HALO - tap_count + 1 + j), 64), :
                ]
            normed_ref[b, pl.ds(start, 64), :] = total
            return carry

        lax.fori_loop(0, length // 64, conv, 0)
    stores = [pltpu.make_async_copy(gated_ref, gated_hbm, out_sems.at[0])]
    stores[0].start()

    def norm(i, carry):
        rows = pl.ds(pl.multiple_of(i * 64, 64), 64)
        parts = [normed_ref[b, rows, :] for b in range(blocks)]
        mean = jnp.sum(sum(parts), axis=-1, keepdims=True) / channels
        centred = [p - mean for p in parts]
        var = jnp.sum(sum(p * p for p in centred), axis=-1, keepdims=True) / channels
        inv = lax.rsqrt(var + epsilon)
        inv_ref[rows, :] = jnp.broadcast_to(inv, (64, LANES))
        for b in range(blocks):
            lanes = slice(b * LANES, (b + 1) * LANES)
            normed = centred[b] * inv
            normed_ref[b, rows, :] = normed
            pre = normed * gain_ref[:, lanes] + shift_ref[:, lanes]
            sig = sigmoid(pre)
            act = pre * sig
            act_ref[rows, lanes] = act.astype(BF16)
            slope_ref[b, rows, :] = sig + act * (1.0 - sig)
        return carry

    lax.fori_loop(0, length // 64, norm, 0)
    for n, pair in enumerate(
        (
            (act_ref, act_hbm), (normed_ref, normed_hbm), (inv_ref, inv_hbm),
            (slope_ref, slope_hbm),
        )
    ):
        store = pltpu.make_async_copy(*pair, out_sems.at[1 + n])
        store.start()
        stores.append(store)
    for store in stores:
        store.wait()


def weight_kernel(
    where_ref, act_hbm, other_act_hbm, cotan_hbm, other_cotan_hbm,
    sent_hbm, kept_hbm,
    act_ref, other_act_ref, cotan_ref, other_cotan_ref, sent_ref, kept_ref, in_sems, out_sems,
):
    wide = sent_ref.shape[1]
    group, me = where_ref[0], where_ref[1]
    loads = [
        pltpu.make_async_copy(act_hbm, act_ref, in_sems.at[0]),
        pltpu.make_async_copy(other_act_hbm, other_act_ref, in_sems.at[1]),
    ]
    for x in range(4):
        columns = pl.ds(pl.multiple_of((2 * x + me) * wide, wide), wide)
        loads.append(
            pltpu.make_async_copy(
                cotan_hbm.at[:, columns], cotan_ref.at[x], in_sems.at[2 + 2 * x]
            )
        )
        loads.append(
            pltpu.make_async_copy(
                other_cotan_hbm.at[:, columns], other_cotan_ref.at[x], in_sems.at[3 + 2 * x]
            )
        )
    for load in loads:
        load.start()
    loads[0].wait()
    loads[1].wait()
    dims = (((0,), (0,)), ((), ()))
    stores = []
    for x in range(4):
        loads[2 + 2 * x].wait()
        loads[3 + 2 * x].wait()
        term = lax.dot_general(
            cotan_ref[x], act_ref[...], dims, preferred_element_type=F32
        ) + lax.dot_general(
            other_cotan_ref[x], other_act_ref[...], dims, preferred_element_type=F32
        )
        sent_ref[x] = term.astype(BF16)

        @pl.when(group == x)
        def _():
            kept_ref[...] = term

        store = pltpu.make_async_copy(sent_ref.at[x], sent_hbm.at[x], out_sems.at[x])
        store.start()
        stores.append(store)
    store = pltpu.make_async_copy(kept_ref, kept_hbm, out_sems.at[4])
    store.start()
    stores.append(store)
    for store in stores:
        store.wait()


def backward_kernel(
    where_ref, gain_ref, normed_hbm, inv_hbm, slope_hbm, gated_hbm, own_hbm, other_hbm, cotan_hbm,
    grad_hbm, head_ref, small_ref,
    normed_ref, inv_ref, slope_ref, gated_ref, own_ref, other_ref, cotan_ref, grad_ref,
    in_sems, out_sem,
):
    length = inv_ref.shape[0]
    blocks = normed_ref.shape[0]
    channels = blocks * LANES
    me = where_ref[1]
    wide = own_ref.shape[1]
    tap_count = 31
    step = 128
    loads = []
    for n, pair in enumerate(
        (
            (own_hbm, own_ref), (cotan_hbm, cotan_ref), (other_hbm, other_ref),
            (normed_hbm, normed_ref), (slope_hbm, slope_ref), (inv_hbm, inv_ref),
            (gated_hbm, gated_ref),
        )
    ):
        load = pltpu.make_async_copy(*pair, in_sems.at[n])
        load.start()
        loads.append(load)
    for load in loads[:3]:
        load.wait()

    def rows_of(i, carry):
        rows = pl.ds(pl.multiple_of(i * step, step), step)
        total = jnp.zeros((step, channels), F32)
        for x in range(4):
            own = pl.ds(pl.multiple_of((2 * x + me) * wide, wide), wide)
            other = pl.ds(pl.multiple_of((2 * x + 1 - me) * wide, wide), wide)
            total = total + jnp.dot(
                cotan_ref[rows, own], own_ref[x], preferred_element_type=F32
            )
            total = total + jnp.dot(
                cotan_ref[rows, other], other_ref[x], preferred_element_type=F32
            )
        for b in range(blocks):
            grad_ref[b, rows, :] = total[:, b * LANES : (b + 1) * LANES]
        return carry

    lax.fori_loop(0, length // step, rows_of, 0)
    for load in loads[3:6]:
        load.wait()

    def point(i, carry):
        rows = pl.ds(pl.multiple_of(i * 32, 32), 32)
        inv = inv_ref[rows, :]
        grads = []
        normeds = []
        gains = []
        shifts = []
        for b in range(blocks):
            lanes = slice(b * LANES, (b + 1) * LANES)
            normed = normed_ref[b, rows, :]
            grad_pre = grad_ref[b, rows, :] * slope_ref[b, rows, :]
            gains.append(carry[b] + jnp.sum((grad_pre * normed).reshape(4, 8, LANES), axis=0))
            shifts.append(carry[blocks + b] + jnp.sum(grad_pre.reshape(4, 8, LANES), axis=0))
            grads.append(grad_pre * gain_ref[:, lanes])
            normeds.append(normed)
        first = jnp.sum(sum(grads), axis=-1, keepdims=True) / channels
        second = (
            jnp.sum(sum(g * n for g, n in zip(grads, normeds)), axis=-1, keepdims=True) / channels
        )
        for b in range(blocks):
            grad_ref[b, rows, :] = inv * (grads[b] - first - normeds[b] * second)
        return tuple(gains + shifts)

    zero = jnp.zeros((8, LANES), F32)
    sums = lax.fori_loop(0, length // 32, point, (zero,) * (2 * blocks))
    store = pltpu.make_async_copy(grad_ref, grad_hbm, out_sem)
    store.start()
    loads[6].wait()
    for b in range(blocks):
        head_ref[b] = grad_ref[b, 0:HALO, :]
        small_ref[b] = jnp.zeros(small_ref.shape[1:], F32)
        small_ref[b, tap_count : tap_count + 1, :] = jnp.sum(sums[b], axis=0, keepdims=True)
        small_ref[b, tap_count + 1 : tap_count + 2, :] = jnp.sum(
            sums[blocks + b], axis=0, keepdims=True
        )

        def taps(i, carry, b=b):
            start = pl.multiple_of(i * 8, 8)
            grad = grad_ref[b, pl.ds(start, 8), :]
            return tuple(
                carry[j]
                + grad * gated_ref[b, pl.ds(start + (HALO - tap_count + 1 + j), 8), :]
                for j in range(tap_count)
            )

        parts = lax.fori_loop(0, length // 8, taps, (zero,) * tap_count, unroll=2)
        for j in range(tap_count):
            small_ref[b, j : j + 1, :] = jnp.sum(parts[j], axis=0, keepdims=True)
    store.wait()


def gated_kernel(
    later_ref, taps_ref, grad_hbm, value_hbm, gate_hbm, out_value_ref, out_gate_ref,
    ext_ref, value_ref, gate_ref, sems,
):
    length, channels = value_ref.shape
    blocks = channels // LANES
    tap_count = taps_ref.shape[0]
    loads = []
    for b in range(blocks):
        loads.append(
            pltpu.make_async_copy(grad_hbm.at[b], ext_ref.at[b, pl.ds(0, length)], sems.at[b])
        )
    loads.append(pltpu.make_async_copy(value_hbm, value_ref, sems.at[blocks]))
    loads.append(pltpu.make_async_copy(gate_hbm, gate_ref, sems.at[blocks + 1]))
    for load in loads:
        load.start()
    for b in range(blocks):
        ext_ref[b, length : length + HALO, :] = later_ref[b]
    for load in loads:
        load.wait()
    for b in range(blocks):
        lanes = slice(b * LANES, (b + 1) * LANES)

        def conv(i, carry, b=b, lanes=lanes):
            start = pl.multiple_of(i * 64, 64)
            rows = pl.ds(start, 64)
            total = jnp.zeros((64, LANES), F32)
            for j in range(tap_count):
                total = total + taps_ref[j : j + 1, lanes] * ext_ref[
                    b, pl.ds(start + (tap_count - 1 - j), 64), :
                ]
            sig = sigmoid(gate_ref[rows, lanes].astype(F32))
            part = total * sig
            out_value_ref[rows, lanes] = part.astype(BF16)
            out_gate_ref[rows, lanes] = (
                part * value_ref[rows, lanes].astype(F32) * (1.0 - sig)
            ).astype(BF16)
            return carry

        lax.fori_loop(0, length // 64, conv, 0)


def pack_kernel(where_ref, parts_ref, kept_ref, small_ref, out_ref):
    count = out_ref.shape[0]
    blocks, small_rows, _ = small_ref.shape
    halves = small_rows // 4
    group = where_ref[0]
    weights = [jnp.where(group == x, 0.0, 1.0) for x in range(4)]
    for i in range(count // 4):
        rows = slice(16 * i, 16 * i + 16)
        tiles = []
        for b in range(blocks):
            lanes = slice(b * LANES, (b + 1) * LANES)
            tiles.append(
                kept_ref[rows, lanes]
                + sum(parts_ref[x, rows, lanes].astype(F32) * weights[x] for x in range(4))
            )
        for k in range(2):
            for h in range(2):
                m = 4 * i + 2 * k + h
                pieces = [tiles[2 * h + t][8 * k : 8 * k + 8] for t in range(2)]
                if m < blocks * halves:
                    b, g = m // halves, m % halves
                    tile = small_ref[b, 4 * g : 4 * g + 4, :]
                    high = tile.astype(BF16).astype(F32)
                    pieces += [high, tile - high]
                else:
                    pieces.append(jnp.zeros((8, LANES), F32))
                out_ref[m] = jnp.concatenate(pieces, axis=0).astype(BF16)


def total_kernel(scale, parts_ref, rows_ref, tiles_ref):
    def add(i, carry):
        return carry + parts_ref[i].astype(F32)

    total = lax.fori_loop(
        0, parts_ref.shape[0], add, jnp.zeros(parts_ref.shape[1:], F32), unroll=8
    ) * scale
    rows_ref[...] = total[0:16]
    tile = jnp.concatenate([total[16:20] + total[20:24], jnp.zeros((4, LANES), F32)], axis=0)
    for i in range(tiles_ref.shape[0]):
        tiles_ref[i] = tile


def spread_kernel(rows_ref, tiles_ref, out_ref):
    tile = sum(tiles_ref[i] for i in range(tiles_ref.shape[0]))[0:4]
    high = tile.astype(BF16).astype(F32)
    both = jnp.concatenate([rows_ref[...], high, tile - high], axis=0).astype(BF16)

    def put(i, carry):
        out_ref[i] = both
        return carry

    lax.fori_loop(0, out_ref.shape[0], put, 0, unroll=8)


def unpack_kernel(parts_ref, weight_ref, taps_ref, gain_ref, shift_ref, small_ref):
    count = parts_ref.shape[0]
    small_rows = small_ref.shape[0]
    tap_count = taps_ref.shape[0]
    blocks = small_ref.shape[1] // LANES
    halves = small_rows // 4
    for m in range(count):
        i, h = m // 2, m % 2
        part = parts_ref[m].astype(F32)
        for t in range(2):
            weight_ref[8 * i : 8 * i + 8, (2 * h + t) * LANES : (2 * h + t + 1) * LANES] = part[
                8 * t : 8 * t + 8
            ]
        if m < blocks * halves:
            b, g = m // halves, m % halves
            small_ref[4 * g : 4 * g + 4, b * LANES : (b + 1) * LANES] = part[16:20] + part[20:24]
    taps_ref[...] = small_ref[0:tap_count, :]
    gain_ref[...] = small_ref[tap_count : tap_count + 1, :]
    shift_ref[...] = small_ref[tap_count + 1 : tap_count + 2, :]


def from_behind(value, axis, by):
    count = lax.axis_size(axis)
    pairs = [(i, i + by) for i in range(count) if 0 <= i + by < count]
    return lax.ppermute(value, axis, pairs)


def swapped(value):
    return lax.ppermute(value, "dp_1", [(0, 1), (1, 0)])


def exchanged(value, axes):
    return lax.all_to_all(value, axes, 0, 0, tiled=True)


def per_device(glu_value, glu_gate, cotangent, conv_weight, norm_gain, norm_shift, out_weight):
    value_rows = glu_value[0]
    gate_rows = glu_gate[0]
    cotan_rows = cotangent[0]
    length, channels = value_rows.shape
    blocks = channels // LANES
    features = cotan_rows.shape[1]
    wide = out_weight.shape[0]
    tap_count = conv_weight.shape[0]
    count_sp = lax.axis_size(SP)
    count_dp = lax.axis_size(DP)
    scale = 1.0 / math.sqrt(length * count_sp * count_dp)
    where = jnp.stack([lax.axis_index("dp_0"), lax.axis_index("dp_1")]).astype(jnp.int32)
    gain = norm_gain.reshape(1, channels)
    shift = norm_shift.reshape(1, channels)
    shaped = jax.ShapeDtypeStruct

    halo = jnp.concatenate([value_rows[length - HALO :], gate_rows[length - HALO :]], axis=0)
    halo = from_behind(halo, SP, 1)
    other_cotan = swapped(cotan_rows)
    own_weight = exchanged(jnp.broadcast_to(out_weight[None], (4, *out_weight.shape)), "dp_0")

    act, normed, inv, slope, gated = pl.pallas_call(
        forward_kernel,
        out_shape=(
            shaped((length, channels), BF16),
            shaped((blocks, length, LANES), F32),
            shaped((length, LANES), F32),
            shaped((blocks, length, LANES), F32),
            shaped((blocks, length + HALO, LANES), F32),
        ),
        in_specs=[VMEM] * 3 + [HBM] * 3,
        out_specs=(HBM,) * 5,
        scratch_shapes=[
            pltpu.VMEM((2 * HALO, channels), BF16),
            pltpu.VMEM((length, channels), BF16),
            pltpu.VMEM((length, channels), BF16),
            pltpu.VMEM((length, channels), BF16),
            pltpu.VMEM((blocks, length, LANES), F32),
            pltpu.VMEM((length, LANES), F32),
            pltpu.VMEM((blocks, length, LANES), F32),
            pltpu.VMEM((blocks, length + HALO, LANES), F32),
            pltpu.SemaphoreType.DMA((3,)),
            pltpu.SemaphoreType.DMA((5,)),
        ],
        compiler_params=params(63),
        cost_estimate=cost(6),
        name="module_forward",
    )(conv_weight, gain, shift, halo, value_rows, gate_rows)
    other_act = swapped(act)
    own_weight, act = lax.optimization_barrier((own_weight, act))
    other_weight = swapped(own_weight)
    sent, kept = pl.pallas_call(
        weight_kernel,
        out_shape=(shaped((4, wide, channels), BF16), shaped((wide, channels), F32)),
        in_specs=[SMEM] + [HBM] * 4,
        out_specs=(HBM,) * 2,
        scratch_shapes=[
            pltpu.VMEM((length, channels), BF16),
            pltpu.VMEM((length, channels), BF16),
            pltpu.VMEM((4, length, wide), BF16),
            pltpu.VMEM((4, length, wide), BF16),
            pltpu.VMEM((4, wide, channels), BF16),
            pltpu.VMEM((wide, channels), F32),
            pltpu.SemaphoreType.DMA((10,)),
            pltpu.SemaphoreType.DMA((5,)),
        ],
        compiler_params=params(63),
        cost_estimate=cost(3),
        name="weight_term",
    )(where, act, other_act, cotan_rows, other_cotan)
    arrived = exchanged(sent, "dp_0")

    small_rows = -(-(tap_count + 2) // 8) * 8
    grad, head, small = pl.pallas_call(
        backward_kernel,
        out_shape=(
            shaped((blocks, length, LANES), F32),
            shaped((blocks, HALO, LANES), F32),
            shaped((blocks, small_rows, LANES), F32),
        ),
        in_specs=[SMEM, VMEM] + [HBM] * 7,
        out_specs=(HBM, VMEM, VMEM),
        scratch_shapes=[
            pltpu.VMEM((blocks, length, LANES), F32),
            pltpu.VMEM((length, LANES), F32),
            pltpu.VMEM((blocks, length, LANES), F32),
            pltpu.VMEM((blocks, length + HALO, LANES), F32),
            pltpu.VMEM((4, wide, channels), BF16),
            pltpu.VMEM((4, wide, channels), BF16),
            pltpu.VMEM((length, features), BF16),
            pltpu.VMEM((blocks, length, LANES), F32),
            pltpu.SemaphoreType.DMA((7,)),
            pltpu.SemaphoreType.DMA,
        ],
        compiler_params=params(63),
        cost_estimate=cost(10),
        name="module_backward",
    )(where, gain, normed, inv, slope, gated, own_weight, other_weight, cotan_rows)
    later = from_behind(head, SP, -1)

    packed = pl.pallas_call(
        pack_kernel,
        out_shape=shaped((count_sp, 24, LANES), BF16),
        in_specs=[SMEM] + [VMEM] * 3,
        out_specs=VMEM,
        compiler_params=params(8),
        cost_estimate=cost(1),
        name="pack",
    )(where, arrived, kept, small)
    packed, later = lax.optimization_barrier((packed, later))
    grad_value, grad_gate = pl.pallas_call(
        gated_kernel,
        out_shape=(shaped((length, channels), BF16), shaped((length, channels), BF16)),
        in_specs=[VMEM] * 2 + [HBM] * 3,
        out_specs=(VMEM,) * 2,
        scratch_shapes=[
            pltpu.VMEM((blocks, length + HALO, LANES), F32),
            pltpu.VMEM((length, channels), BF16),
            pltpu.VMEM((length, channels), BF16),
            pltpu.SemaphoreType.DMA((blocks + 2,)),
        ],
        compiler_params=params(63),
        cost_estimate=cost(6),
        name="gated_backward",
    )(later, conv_weight, grad, value_rows, gate_rows)

    terms = exchanged(packed, SP)
    rows, tiles = pl.pallas_call(
        functools.partial(total_kernel, scale),
        out_shape=(shaped((16, LANES), F32), shaped((count_dp, 8, LANES), F32)),
        in_specs=[VMEM],
        out_specs=(VMEM,) * 2,
        compiler_params=params(4),
        cost_estimate=cost(1),
        name="total",
    )(terms)
    tiles = exchanged(tiles, DP)
    totals = pl.pallas_call(
        spread_kernel,
        out_shape=shaped((count_sp, 24, LANES), BF16),
        in_specs=[VMEM] * 2,
        out_specs=VMEM,
        compiler_params=params(4),
        cost_estimate=cost(1),
        name="spread",
    )(rows, tiles)
    whole = exchanged(totals, SP)
    grad_out_weight, grad_conv, grad_gain, grad_shift = pl.pallas_call(
        unpack_kernel,
        out_shape=(
            shaped((wide, channels), F32),
            shaped((tap_count, channels), F32),
            shaped((1, channels), F32),
            shaped((1, channels), F32),
        ),
        in_specs=[VMEM],
        out_specs=(VMEM,) * 4,
        scratch_shapes=[pltpu.VMEM((small_rows, channels), F32)],
        compiler_params=params(8),
        cost_estimate=cost(1),
        name="unpack",
    )(whole)
    return (
        grad_value[None],
        grad_gate[None],
        grad_out_weight,
        grad_conv,
        grad_gain.reshape(channels),
        grad_shift.reshape(channels),
    )


def solution(mesh):
    split = Mesh(mesh.devices.reshape(8, 8, 4, 2), ("sp_0", "sp_1", "dp_0", "dp_1"))
    return jax.shard_map(
        per_device,
        mesh=split,
        in_specs=(P(DP, SP, None), P(DP, SP, None), P(DP, SP, None), P(), P(), P(), P(DP, None)),
        out_specs=(P(DP, SP, None), P(DP, SP, None), P(DP, None), P(), P(), P()),
        check_vma=False,
    )
```

time: 393 us -> 127 us (0.32)
  waiting for transfers between devices: 239 us -> 16.8 us
  other arithmetic: 37.9 us -> 0.66 us
  Pallas kernels: 0 us -> 34.4 us
  local copies, waits for them, and re-layouts: 33.2 us -> 5.11 us
  blocking collectives: 17.3 us -> 38.3 us
  starting transfers between devices: 44.9 us -> 29.2 us
  between operations: 14 us -> 0.79 us
  matrix products: 5.23 us -> 0 us
    psum x4 -> x0, waiting for transfers between devices: 214 us -> none  [over_axes(): return functools.reduce(lax.psum, axes, value)]
    pallas_call x0 -> x8, Pallas kernels: none -> 34.4 us  [the longest x1 10.7 us: per_device(): pl.pallas_call(backward_kernel, out_shape=(shaped((blocks, length, LANES)...]
    all_to_all x4 -> x3, starting transfers between devices: 36.2 us -> 13.1 us  [exchanged(): return lax.all_to_all(value, axes, 0, 0, tiled=True)]
    all_to_all x2, blocking collectives: 17.3 us -> 38.3 us  [exchanged(): return lax.all_to_all(value, axes, 0, 0, tiled=True)]
    reduce_sum x7 -> x0, other arithmetic: 20.7 us -> none  [the longest x2 6.7 us: per_device(): jnp.sum(grad_conv_rows * gated_ext[offset:offset + length], axis=0)]
    ppermute x0 -> x3, starting transfers between devices: none -> 13.4 us  [swapped(): return lax.ppermute(value, 'dp_1', [(0, 1), (1, 0)])]
    all_to_all x4 -> x3, waiting for transfers between devices: 24.7 us -> 13.7 us  [exchanged(): return lax.all_to_all(value, axes, 0, 0, tiled=True)]
    another operation x3 -> x0, local copies, waits for them, and re-layouts: 9.99 us -> none  [the longest x2 9.84 us: cut_along(): return jnp.moveaxis(value.reshape(*before, count, -1, *after), dim, 0)]
  transfers between devices with their start and end apart: 11 -> 8, of which waited for: 6 -> 5; matrix products, arithmetic and copies ran while one was open for 11% -> 3% of each run, Pallas kernels for 0% -> 26%
where the time goes in v1:
time: 127 us; the launch traced here: 125 us
  blocking collectives  38.3 us (30%)
  Pallas kernels  34.4 us (27%)
  starting transfers between devices  29.2 us (23%)
  waiting for transfers between devices  16.8 us (13%)
  local copies, waits for them, and re-layouts  5.11 us (4%)
    all_to_all x2, blocking collectives, exchanged(): return lax.all_to_all(value, axes, 0, 0, tiled=True)  38.3 us
    all_to_all x3, waiting for transfers between devices, exchanged(): return lax.all_to_all(value, axes, 0, 0, tiled=True)  13.7 us
    ppermute x3, starting transfers between devices, swapped(): return lax.ppermute(value, 'dp_1', [(0, 1), (1, 0)])  13.4 us
    all_to_all x3, starting transfers between devices, exchanged(): return lax.all_to_all(value, axes, 0, 0, tiled=True)  13.1 us
    pallas_call x1, Pallas kernels, per_device(): pl.pallas_call(backward_kernel, out_shape=(shaped((blocks, length, LANES)...  10.7 us
    pallas_call x1, Pallas kernels, per_device(): pl.pallas_call(forward_kernel, out_shape=(shaped((length, channels), BF16...  8.83 us
    pallas_call x1, Pallas kernels, per_device(): pl.pallas_call(gated_kernel, out_shape=(shaped((length, channels), BF16),...  6.66 us
    pallas_call x1, Pallas kernels, per_device(): pl.pallas_call(weight_kernel, out_shape=(shaped((4, wide, channels), BF16...  4.93 us
  transfers between devices with their start and end apart: 8, of which 5 were waited for; matrix products, arithmetic and copies ran while one was open for 3% of the time, Pallas kernels for 26%

profile of v1, /device:TPU:1, one launch (start us, length us, event | category | flops | bytes accessed | tf_op | source)
XLA Modules:
  0.0 125.2 jit_solution(11751211570499923629)
XLA Ops:
  0.6 8.8 %collective-permute-start.2 = (bf16[512,2048]{1,0:T(8,128)(2,1)}, bf16[512,2048]{1,0:T(8,128)(2,1)}, u32[]{:S(2)}, u32[]{:S(2)}) collective-permute-start(bf16[512,2048]{1,0:T(8,128)(2,1)} %bitcast.19), channel_id=1, source_target_pairs={{0,1},{1,0},{2,3},{3,2},{4,5},{5,4},{6,7},{7,6},{8,9},{9,8},{10,11... | collective-permute-start | bytes 6291464 | tf_op jit(solution)/shard_map/ppermute | solution.py:393
  9.4 2.0 %broadcast_in_dim.12 = bf16[4,256,512]{2,1,0:T(8,128)(2,1)} broadcast(bf16[256,512]{1,0:T(8,128)(2,1)} %param.13), dimensions={1,2} | broadcast | bytes 1310720 | tf_op jit(solution)/shard_map/broadcast_in_dim | solution.py:420
  11.4 4.3 %all-to-all-start = ((bf16[4,256,512]{2,1,0:T(8,128)(2,1)}), bf16[4,256,512]{2,1,0:T(8,128)(2,1)}, u32[]{:S(2)}, u32[]{:S(2)}) async-start(bf16[4,256,512]{2,1,0:T(8,128)(2,1)} %broadcast_in_dim.12), calls=%async_computation | async-start | bytes 2097152 | tf_op jit(solution)/shard_map/all_to_all | solution.py:397
  15.7 0.8 slice_bitcast_fusion
  16.5 1.3 %collective-permute-start = (bf16[64,512]{1,0:T(8,128)(2,1)S(1)}, bf16[64,512]{1,0:T(8,128)(2,1)S(1)}, u32[]{:S(2)}, u32[]{:S(2)}) collective-permute-start(bf16[64,512]{1,0:T(8,128)(2,1)S(1)} %pad_maximum_fusion), channel_id=1, source_target_pairs={{0,8},{8,16},{16,24},{24,32},{32,40},{40,48},{48,56},{56,64},{64,7... | collective-permute-start | bytes 196616 | tf_op jit(solution)/shard_map/ppermute | solution.py:389
  17.8 1.7 %collective-permute-done.halo_hbm = bf16[64,512]{1,0:T(8,128)(2,1)S(1)} collective-permute-done((bf16[64,512]{1,0:T(8,128)(2,1)S(1)}, bf16[64,512]{1,0:T(8,128)(2,1)S(1)}, u32[]{:S(2)}, u32[]{:S(2)}) %collective-permute-start) | collective-permute-done | bytes 65568 | tf_op jit(solution)/shard_map/ppermute | solution.py:389
  19.4 0.0 copy-start.5
  19.4 0.6 copy-done.5
  20.1 8.8 %module_forward.1 = (bf16[512,512]{1,0:T(8,128)(2,1)}, f32[4,512,128]{2,1,0:T(8,128)}, f32[512,128]{1,0:T(8,128)}, f32[4,512,128]{2,1,0:T(8,128)}, f32[4,544,128]{2,1,0:T(8,128)}) custom-call(f32[31,512]{1,0:T(8,128)} %taps_ref.3, f32[1,512]{1,0:T(1,128)} %bitcast.23, f32[1,512]{1,0:T(1,128)} %bitcast.22, bf16[64,512]{1,0:T(8,128)(2,1)} %copy-done.5, ...), custom_call_target="tpu_custom_call" | custom-call | flops 3000000000 | bytes 1048576 | tf_op jit(solution)/shard_map/module_forward/pallas_call | solution.py:422
  28.9 2.0 %all-to-all-done.own_hbm = bf16[4,256,512]{2,1,0:T(8,128)(2,1)} async-done(((bf16[4,256,512]{2,1,0:T(8,128)(2,1)}), bf16[4,256,512]{2,1,0:T(8,128)(2,1)}, u32[]{:S(2)}, u32[]{:S(2)}) %all-to-all-start) | async-done | bytes 1048608 | tf_op jit(solution)/shard_map/all_to_all | solution.py:397
  30.9 2.8 %collective-permute-start.3 = (bf16[4,256,512]{2,1,0:T(8,128)(2,1)}, bf16[4,256,512]{2,1,0:T(8,128)(2,1)}, u32[]{:S(2)}, u32[]{:S(2)}) collective-permute-start(bf16[4,256,512]{2,1,0:T(8,128)(2,1)} %all-to-all-done.own_hbm), channel_id=1, source_target_pairs={{0,1},{1,0},{2,3},{3,2},{4,5},{5,4},{6,7},{7,6},{8,9},{9,8},{10,11... | collective-permute-start | bytes 3145736 | tf_op jit(solution)/shard_map/ppermute | solution.py:393
  33.7 1.9 %collective-permute-start.1 = (bf16[512,512]{1,0:T(8,128)(2,1)}, bf16[512,512]{1,0:T(8,128)(2,1)S(1)}, u32[]{:S(2)}, u32[]{:S(2)}) collective-permute-start(bf16[512,512]{1,0:T(8,128)(2,1)} %get-tuple-element.29.act_hbm), channel_id=1, source_target_pairs={{0,1},{1,0},{2,3},{3,2},{4,5},{5,4},{6,7},{7,6},{8,9},{9,8},{10,11... | collective-permute-start | bytes 1572872 | tf_op jit(solution)/shard_map/ppermute | solution.py:393
  35.6 0.7 pad_add_fusion.where_ref
  36.3 1.4 %collective-permute-done.1.other_act_hbm = bf16[512,512]{1,0:T(8,128)(2,1)S(1)} collective-permute-done((bf16[512,512]{1,0:T(8,128)(2,1)}, bf16[512,512]{1,0:T(8,128)(2,1)S(1)}, u32[]{:S(2)}, u32[]{:S(2)}) %collective-permute-start.1) | collective-permute-done | bytes 524320 | tf_op jit(solution)/shard_map/ppermute | solution.py:393
  37.7 0.0 copy-start.3
  37.7 0.0 collective-permute-done.2.other_cotan_hbm
  37.7 0.8 copy-done.3
  38.5 4.9 %weight_term.1 = (bf16[4,256,512]{2,1,0:T(8,128)(2,1)}, f32[256,512]{1,0:T(8,128)}) custom-call(s32[2]{0:T(128)} %pad_add_fusion.where_ref, bf16[512,512]{1,0:T(8,128)(2,1)} %get-tuple-element.29.act_hbm, bf16[512,512]{1,0:T(8,128)(2,1)} %copy-done.3, bf16[512,2048]{1,0:T(8,128)(2,1)} %bitcast.20, bf16[512,2048]{1,0:T(8,128)(2,1)} %collective-permute-done.2.other_cotan_hbm), custom_call_target="tpu_custom_call" | custom-call | flops 1500000000 | bytes 1048576 | tf_op jit(solution)/shard_map/weight_term/pallas_call | solution.py:452
  43.4 4.3 %all-to-all-start.1 = ((bf16[4,256,512]{2,1,0:T(8,128)(2,1)}), bf16[4,256,512]{2,1,0:T(8,128)(2,1)}, u32[]{:S(2)}, u32[]{:S(2)}) async-start(bf16[4,256,512]{2,1,0:T(8,128)(2,1)} %get-tuple-element.30), calls=%async_computation.1 | async-start | bytes 2097152 | tf_op jit(solution)/shard_map/all_to_all | solution.py:397
  47.7 0.0 collective-permute-done.3.other_hbm
  47.7 0.0 copy-start
  47.7 0.0 copy-start.2
  47.7 10.7 %module_backward.1 = (f32[4,512,128]{2,1,0:T(8,128)}, f32[4,32,128]{2,1,0:T(8,128)}, f32[4,40,128]{2,1,0:T(8,128)}) custom-call(s32[2]{0:T(128)} %pad_add_fusion.where_ref, f32[1,512]{1,0:T(1,128)} %bitcast.24, f32[4,512,128]{2,1,0:T(8,128)} %get-tuple-element.32.normed_hbm, f32[512,128]{1,0:T(8,128)} %get-tuple-element.33.inv_hbm, ...), custom_call_target="tpu_custom_call" | custom-call | flops 5000000000 | bytes 1048576 | tf_op jit(solution)/shard_map/module_backward/pallas_call | solution.py:474
  58.4 1.3 %collective-permute-start.4 = (f32[4,32,128]{2,1,0:T(8,128)}, f32[4,32,128]{2,1,0:T(8,128)S(1)}, u32[]{:S(2)}, u32[]{:S(2)}) collective-permute-start(f32[4,32,128]{2,1,0:T(8,128)} %get-tuple-element.38), channel_id=1, source_target_pairs={{8,0},{16,8},{24,16},{32,24},{40,32},{48,40},{56,48},{64,56},{72,6... | collective-permute-start | bytes 196616 | tf_op jit(solution)/shard_map/ppermute | solution.py:389
  59.7 3.1 %all-to-all-done.1.parts_ref = bf16[4,256,512]{2,1,0:T(8,128)(2,1)} async-done(((bf16[4,256,512]{2,1,0:T(8,128)(2,1)}), bf16[4,256,512]{2,1,0:T(8,128)(2,1)}, u32[]{:S(2)}, u32[]{:S(2)}) %all-to-all-start.1) | async-done | bytes 1048608 | tf_op jit(solution)/shard_map/all_to_all | solution.py:397
  62.8 0.0 copy-done
  62.8 0.0 copy-done.2
  62.8 0.0 copy-start.1
  62.8 0.9 copy-done.1
  63.7 1.5 %pack.1 = bf16[64,24,128]{2,1,0:T(8,128)(2,1)S(1)} custom-call(s32[2]{0:T(128)S(1)} %copy-done.2, bf16[4,256,512]{2,1,0:T(8,128)(2,1)} %all-to-all-done.1.parts_ref, f32[256,512]{1,0:T(8,128)S(1)} %copy-done, f32[4,40,128]{2,1,0:T(8,128)S(1)} %copy-done.1), custom_call_target="tpu_custom_call" | custom-call | flops 500000000 | bytes 1048576 | tf_op jit(solution)/shard_map/pack/pallas_call | solution.py:501
  65.2 0.0 collective-permute-done.4.later_ref
  65.2 0.0 copy-start.4
  65.2 26.6 %all_to_all.25.parts_ref = bf16[64,24,128]{2,1,0:T(8,128)(2,1)S(1)} all-to-all(bf16[64,24,128]{2,1,0:T(8,128)(2,1)S(1)} %pack.1), channel_id=1, replica_groups=mesh['sp_0'=8,'sp_1'=8,'dp_0'=4,'dp_1'=2] {'sp_0','sp_1'}, dimensions={0} | all-to-all | bytes 786432 | tf_op jit(solution)/shard_map/all_to_all | solution.py:397
  91.8 0.1 total.1
  91.9 11.7 %all_to_all.26.tiles_ref = f32[8,8,128]{2,1,0:T(8,128)S(1)} all-to-all(f32[8,8,128]{2,1,0:T(8,128)S(1)} %get-tuple-element.45), channel_id=1, replica_groups=mesh['sp_0'=8,'sp_1'=8,'dp_0'=4,'dp_1'=2] {'dp_0','dp_1'}, dimensions={0} | all-to-all | bytes 65536 | tf_op jit(solution)/shard_map/all_to_all | solution.py:397
  103.6 0.8 spread.1
  104.4 0.0 copy-done.4
  104.4 4.6 %all-to-all-start.4 = ((bf16[64,24,128]{2,1,0:T(8,128)(2,1)}), bf16[64,24,128]{2,1,0:T(8,128)(2,1)S(1)}, u32[]{:S(2)}, u32[]{:S(2)}) async-start(bf16[64,24,128]{2,1,0:T(8,128)(2,1)} %spread.1), calls=%async_computation.4 | async-start | bytes 786432 | tf_op jit(solution)/shard_map/all_to_all | solution.py:397
  109.1 6.7 %gated_backward.1 = (bf16[512,512]{1,0:T(8,128)(2,1)}, bf16[512,512]{1,0:T(8,128)(2,1)}) custom-call(f32[4,32,128]{2,1,0:T(8,128)} %copy-done.4, f32[31,512]{1,0:T(8,128)} %taps_ref.3, f32[4,512,128]{2,1,0:T(8,128)} %get-tuple-element.40.grad_hbm, bf16[512,512]{1,0:T(8,128)(2,1)} %bitcast.18, bf16[512,512]{1,0:T(8,128)(2,1)} %bitcast.16), custom_call_target="tpu_custom_call" | custom-call | flops 3000000000 | bytes 1048576 | tf_op jit(solution)/shard_map/gated_backward/pallas_call | solution.py:511
  115.8 8.6 %all-to-all-done.4.parts_ref = bf16[64,24,128]{2,1,0:T(8,128)(2,1)S(1)} async-done(((bf16[64,24,128]{2,1,0:T(8,128)(2,1)}), bf16[64,24,128]{2,1,0:T(8,128)(2,1)S(1)}, u32[]{:S(2)}, u32[]{:S(2)}) %all-to-all-start.4) | async-done | bytes 393248 | tf_op jit(solution)/shard_map/all_to_all | solution.py:397
  124.4 0.9 unpack.1
  (1 shorter events, 0.0 us)
Async XLA Ops:
  0.6 37.1 %collective-permute-start.2 = (bf16[512,2048]{1,0:T(8,128)(2,1)}, bf16[512,2048]{1,0:T(8,128)(2,1)}, u32[]{:S(2)}, u32[]{:S(2)}) collective-permute-start(bf16[512,2048]{1,0:T(8,128)(2,1)} %bitcast.19), channel_id=1, source_target_pairs={{0,1},{1,0},{2,3},{3,2},{4,5},{5,4},{6,7},{7,6},{8,9},{9,8},{10,11... | collective-permute-start | bytes 6291464 | tf_op jit(solution)/shard_map/ppermute | solution.py:393
  11.4 19.5 %all-to-all-start = ((bf16[4,256,512]{2,1,0:T(8,128)(2,1)}), bf16[4,256,512]{2,1,0:T(8,128)(2,1)}, u32[]{:S(2)}, u32[]{:S(2)}) async-start(bf16[4,256,512]{2,1,0:T(8,128)(2,1)} %broadcast_in_dim.12), calls=%async_computation | async-start | bytes 2097152 | tf_op jit(solution)/shard_map/all_to_all | solution.py:397
  16.5 3.0 %collective-permute-start = (bf16[64,512]{1,0:T(8,128)(2,1)S(1)}, bf16[64,512]{1,0:T(8,128)(2,1)S(1)}, u32[]{:S(2)}, u32[]{:S(2)}) collective-permute-start(bf16[64,512]{1,0:T(8,128)(2,1)S(1)} %pad_maximum_fusion), channel_id=1, source_target_pairs={{0,8},{8,16},{16,24},{24,32},{32,40},{40,48},{48,56},{56,64},{64,7... | collective-permute-start | bytes 196616 | tf_op jit(solution)/shard_map/ppermute | solution.py:389
  19.4 0.6 copy-start.5
  30.9 16.8 %collective-permute-start.3 = (bf16[4,256,512]{2,1,0:T(8,128)(2,1)}, bf16[4,256,512]{2,1,0:T(8,128)(2,1)}, u32[]{:S(2)}, u32[]{:S(2)}) collective-permute-start(bf16[4,256,512]{2,1,0:T(8,128)(2,1)} %all-to-all-done.own_hbm), channel_id=1, source_target_pairs={{0,1},{1,0},{2,3},{3,2},{4,5},{5,4},{6,7},{7,6},{8,9},{9,8},{10,11... | collective-permute-start | bytes 3145736 | tf_op jit(solution)/shard_map/ppermute | solution.py:393
  33.7 4.0 %collective-permute-start.1 = (bf16[512,512]{1,0:T(8,128)(2,1)}, bf16[512,512]{1,0:T(8,128)(2,1)S(1)}, u32[]{:S(2)}, u32[]{:S(2)}) collective-permute-start(bf16[512,512]{1,0:T(8,128)(2,1)} %get-tuple-element.29.act_hbm), channel_id=1, source_target_pairs={{0,1},{1,0},{2,3},{3,2},{4,5},{5,4},{6,7},{7,6},{8,9},{9,8},{10,11... | collective-permute-start | bytes 1572872 | tf_op jit(solution)/shard_map/ppermute | solution.py:393
  37.7 0.8 copy-start.3
  43.4 19.4 %all-to-all-start.1 = ((bf16[4,256,512]{2,1,0:T(8,128)(2,1)}), bf16[4,256,512]{2,1,0:T(8,128)(2,1)}, u32[]{:S(2)}, u32[]{:S(2)}) async-start(bf16[4,256,512]{2,1,0:T(8,128)(2,1)} %get-tuple-element.30), calls=%async_computation.1 | async-start | bytes 2097152 | tf_op jit(solution)/shard_map/all_to_all | solution.py:397
  47.7 15.1 %copy-start = (f32[256,512]{1,0:T(8,128)S(1)}, f32[256,512]{1,0:T(8,128)}, u32[]{:S(2)}) copy-start(f32[256,512]{1,0:T(8,128)} %get-tuple-element.31.kept_ref) | copy-start | bytes 1572868
  47.7 15.1 %copy-start.2 = (s32[2]{0:T(128)S(1)}, s32[2]{0:T(128)}, u32[]{:S(2)}) copy-start(s32[2]{0:T(128)} %pad_add_fusion.where_ref) | copy-start | bytes 28
  58.4 6.7 %collective-permute-start.4 = (f32[4,32,128]{2,1,0:T(8,128)}, f32[4,32,128]{2,1,0:T(8,128)S(1)}, u32[]{:S(2)}, u32[]{:S(2)}) collective-permute-start(f32[4,32,128]{2,1,0:T(8,128)} %get-tuple-element.38), channel_id=1, source_target_pairs={{8,0},{16,8},{24,16},{32,24},{40,32},{48,40},{56,48},{64,56},{72,6... | collective-permute-start | bytes 196616 | tf_op jit(solution)/shard_map/ppermute | solution.py:389
  62.8 0.9 copy-start.1
  65.2 39.3 %copy-start.4 = (f32[4,32,128]{2,1,0:T(8,128)}, f32[4,32,128]{2,1,0:T(8,128)S(1)}, u32[]{:S(2)}) copy-start(f32[4,32,128]{2,1,0:T(8,128)S(1)} %collective-permute-done.4.later_ref) | copy-start | bytes 196612
  104.4 19.9 %all-to-all-start.4 = ((bf16[64,24,128]{2,1,0:T(8,128)(2,1)}), bf16[64,24,128]{2,1,0:T(8,128)(2,1)S(1)}, u32[]{:S(2)}, u32[]{:S(2)}) async-start(bf16[64,24,128]{2,1,0:T(8,128)(2,1)} %spread.1), calls=%async_computation.4 | async-start | bytes 786432 | tf_op jit(solution)/shard_map/all_to_all | solution.py:397

commit v2 on v1

v2 whole, which is shorter than its diff:
```python
import functools
import math

import jax
import jax.numpy as jnp
from jax import lax
from jax.experimental import pallas as pl
from jax.experimental.pallas import tpu as pltpu
from jax.sharding import Mesh
from jax.sharding import PartitionSpec as P


SP = ("sp_0", "sp_1")
DP = ("dp_0", "dp_1")

epsilon = 1e-06

LANES = 128
HALO = 32
BF16 = jnp.bfloat16
F32 = jnp.float32
VMEM = pl.BlockSpec(memory_space=pltpu.VMEM)
HBM = pl.BlockSpec(memory_space=pltpu.HBM)


def params(mib=16):
    return pltpu.CompilerParams(vmem_limit_bytes=mib * 1024 * 1024)


def cost(us):
    return pl.CostEstimate(flops=int(us * 5.0e8), bytes_accessed=1 << 20, transcendentals=0)


def sigmoid(x):
    return 0.5 * jnp.tanh(0.5 * x) + 0.5


def convolved(load, weights, groups):
    totals = [None] * groups
    for o in range(8 * (groups - 1) + len(weights)):
        rows = load(o)
        for q in range(groups):
            j = o - 8 * q
            if 0 <= j < len(weights):
                term = weights[j] * rows
                totals[q] = term if totals[q] is None else totals[q] + term
    return totals


def prepare_kernel(value_hbm, gate_hbm, weight_hbm, halo_ref, copies_hbm, weight_ref, sems):
    length = value_hbm.shape[0]
    tail = pl.ds(length - HALO, HALO)
    loads = [
        pltpu.make_async_copy(weight_hbm, weight_ref, sems.at[0]),
        pltpu.make_async_copy(value_hbm.at[tail], halo_ref.at[pl.ds(0, HALO)], sems.at[1]),
        pltpu.make_async_copy(gate_hbm.at[tail], halo_ref.at[pl.ds(HALO, HALO)], sems.at[2]),
    ]
    for load in loads:
        load.start()
    loads[0].wait()
    stores = [
        pltpu.make_async_copy(weight_ref, copies_hbm.at[x], sems.at[3 + x]) for x in range(4)
    ]
    for store in stores:
        store.start()
    for copy in loads[1:] + stores:
        copy.wait()


def forward_kernel(
    taps_ref, gain_ref, shift_ref, halo_ref, value_ref, gate_ref,
    act_ref, normed_hbm, inv_hbm,
    normed_ref, inv_ref, gated_ref, out_sems,
):
    length, channels = value_ref.shape
    blocks = channels // LANES
    tap_count = taps_ref.shape[0]
    step = 64
    steps = length // step

    def row_stores(i):
        rows = pl.ds(pl.multiple_of(i * step, step), step)
        return [
            pltpu.make_async_copy(inv_ref.at[rows], inv_hbm.at[rows], out_sems.at[0, i]),
            pltpu.make_async_copy(
                normed_ref.at[:, rows], normed_hbm.at[:, rows], out_sems.at[1, i]
            ),
        ]

    for b in range(blocks):
        lanes = slice(b * LANES, (b + 1) * LANES)
        gated_ref[b, 0:HALO, :] = halo_ref[0:HALO, lanes].astype(F32) * sigmoid(
            halo_ref[HALO : 2 * HALO, lanes].astype(F32)
        )

    def group(i, carry):
        start = pl.multiple_of(i * step, step)
        rows = pl.ds(start, step)
        for b in range(blocks):
            lanes = slice(b * LANES, (b + 1) * LANES)
            gated_ref[b, pl.ds(pl.multiple_of(HALO + start, 32), step), :] = value_ref[
                rows, lanes
            ].astype(F32) * sigmoid(gate_ref[rows, lanes].astype(F32))
        for b in range(blocks):
            lanes = slice(b * LANES, (b + 1) * LANES)
            totals = convolved(
                lambda o: gated_ref[b, pl.ds(start + (HALO - tap_count + 1 + o), 8), :],
                [
                    jnp.broadcast_to(taps_ref[j : j + 1, lanes], (8, LANES))
                    for j in range(tap_count)
                ],
                step // 8,
            )
            for q, total in enumerate(totals):
                normed_ref[b, pl.ds(pl.multiple_of(start + 8 * q, 8), 8), :] = total
        parts = [normed_ref[b, rows, :] for b in range(blocks)]
        mean = jnp.sum(sum(parts), axis=-1, keepdims=True) / channels
        centred = [p - mean for p in parts]
        var = jnp.sum(sum(p * p for p in centred), axis=-1, keepdims=True) / channels
        inv = lax.rsqrt(var + epsilon)
        inv_ref[rows, :] = jnp.broadcast_to(inv, (step, LANES))
        for b in range(blocks):
            lanes = slice(b * LANES, (b + 1) * LANES)
            normed = centred[b] * inv
            normed_ref[b, rows, :] = normed
            pre = normed * gain_ref[:, lanes] + shift_ref[:, lanes]
            act_ref[rows, lanes] = (pre * sigmoid(pre)).astype(BF16)
        for store in row_stores(i):
            store.start()
        return carry

    lax.fori_loop(0, steps, group, 0)
    for i in range(steps):
        for store in row_stores(i):
            store.wait()


def weight_kernel(
    act_ref, other_act_ref, cotan_ref, other_cotan_ref, sent_hbm, kept_hbm,
    sent_ref, kept_ref, out_sems,
):
    wide = sent_ref.shape[1]
    group, me = lax.axis_index("dp_0"), lax.axis_index("dp_1")
    dims = (((0,), (0,)), ((), ()))
    stores = []
    for k in range(4):
        x = lax.rem(group + k, 4)
        columns = pl.ds(pl.multiple_of((2 * x + me) * wide, wide), wide)
        term = lax.dot_general(
            cotan_ref[:, columns], act_ref[...], dims, preferred_element_type=F32
        ) + lax.dot_general(
            other_cotan_ref[:, columns], other_act_ref[...], dims, preferred_element_type=F32
        )
        sent_ref[k] = term.astype(BF16)
        if k == 0:
            kept_ref[...] = term
            stores.append(pltpu.make_async_copy(kept_ref, kept_hbm, out_sems.at[4]))
            stores[-1].start()
        stores.append(pltpu.make_async_copy(sent_ref.at[k], sent_hbm.at[x], out_sems.at[k]))
        stores[-1].start()
    for store in stores:
        store.wait()


def backward_kernel(
    gain_hbm, shift_hbm, normed_hbm, inv_hbm, halo_hbm, value_hbm, gate_hbm, own_hbm, other_ref,
    cotan_hbm,
    grad_hbm, head_ref, small_ref,
    gain_ref, shift_ref, normed_ref, inv_ref, halo_ref, value_ref, gate_ref, own_ref,
    cotan_ref, grad_ref, gated_ref, cotan_sems, in_sems, out_sem,
):
    length = inv_ref.shape[0]
    blocks = normed_ref.shape[0]
    channels = blocks * LANES
    me = lax.axis_index("dp_1")
    wide = own_ref.shape[1]
    tap_count = 31
    step = 128
    columns = [
        pltpu.make_async_copy(
            cotan_hbm.at[:, pl.ds(pl.multiple_of((2 * x + parity) * wide, wide), wide)],
            cotan_ref.at[4 * n + x],
            cotan_sems.at[4 * n + x],
        )
        for n, parity in enumerate((me, 1 - me))
        for x in range(4)
    ]
    own, *rest = [
        pltpu.make_async_copy(source, target, in_sems.at[n])
        for n, (source, target) in enumerate(
            (
                (own_hbm, own_ref), (gain_hbm, gain_ref),
                (shift_hbm, shift_ref), (normed_hbm, normed_ref), (inv_hbm, inv_ref),
                (halo_hbm, halo_ref), (value_hbm, value_ref), (gate_hbm, gate_ref),
            )
        )
    ]
    for load in (*rest[4:], own, *columns, *rest[:4]):
        load.start()

    def half(n, weight_ref):
        def rows_of(i, carry):
            rows = pl.ds(pl.multiple_of(i * step, step), step)
            total = jnp.dot(cotan_ref[4 * n, rows], weight_ref[0], preferred_element_type=F32)
            for x in range(1, 4):
                total = total + jnp.dot(
                    cotan_ref[4 * n + x, rows], weight_ref[x], preferred_element_type=F32
                )
            for b in range(blocks):
                part = total[:, b * LANES : (b + 1) * LANES]
                grad_ref[b, rows, :] = part + grad_ref[b, rows, :] if n else part
            return carry

        lax.fori_loop(0, length // step, rows_of, 0)

    for load in rest[4:]:
        load.wait()
    for b in range(blocks):
        lanes = slice(b * LANES, (b + 1) * LANES)
        gated_ref[b, 0:HALO, :] = halo_ref[0:HALO, lanes].astype(F32) * sigmoid(
            halo_ref[HALO : 2 * HALO, lanes].astype(F32)
        )

        def gating(i, carry, b=b, lanes=lanes):
            rows = pl.ds(pl.multiple_of(i * 64, 64), 64)
            gated_ref[b, pl.ds(pl.multiple_of(HALO + i * 64, 32), 64), :] = value_ref[
                rows, lanes
            ].astype(F32) * sigmoid(gate_ref[rows, lanes].astype(F32))
            return carry

        lax.fori_loop(0, length // 64, gating, 0)

    for load in (own, *columns[:4]):
        load.wait()
    half(0, own_ref)
    for load in columns[4:]:
        load.wait()
    half(1, other_ref)
    for load in rest[:4]:
        load.wait()

    def point(i, carry):
        rows = pl.ds(pl.multiple_of(i * 32, 32), 32)
        inv = inv_ref[rows, :]
        grads = []
        normeds = []
        gains = []
        shifts = []
        for b in range(blocks):
            lanes = slice(b * LANES, (b + 1) * LANES)
            normed = normed_ref[b, rows, :]
            pre = normed * gain_ref[:, lanes] + shift_ref[:, lanes]
            sig = sigmoid(pre)
            grad_pre = grad_ref[b, rows, :] * (sig + pre * sig * (1.0 - sig))
            gains.append(carry[b] + jnp.sum((grad_pre * normed).reshape(4, 8, LANES), axis=0))
            shifts.append(carry[blocks + b] + jnp.sum(grad_pre.reshape(4, 8, LANES), axis=0))
            grads.append(grad_pre * gain_ref[:, lanes])
            normeds.append(normed)
        first = jnp.sum(sum(grads), axis=-1, keepdims=True) / channels
        second = (
            jnp.sum(sum(g * n for g, n in zip(grads, normeds)), axis=-1, keepdims=True) / channels
        )
        for b in range(blocks):
            grad_ref[b, rows, :] = inv * (grads[b] - first - normeds[b] * second)
        return tuple(gains + shifts)

    zero = jnp.zeros((8, LANES), F32)
    sums = lax.fori_loop(0, length // 32, point, (zero,) * (2 * blocks))
    store = pltpu.make_async_copy(grad_ref, grad_hbm, out_sem)
    store.start()
    for b in range(blocks):
        head_ref[b] = grad_ref[b, 0:HALO, :]
        small_ref[b] = jnp.zeros(small_ref.shape[1:], F32)
        small_ref[b, tap_count : tap_count + 1, :] = jnp.sum(sums[b], axis=0, keepdims=True)
        small_ref[b, tap_count + 1 : tap_count + 2, :] = jnp.sum(
            sums[blocks + b], axis=0, keepdims=True
        )

        def taps(i, carry, b=b):
            start = pl.multiple_of(i * 32, 32)
            grads = [
                grad_ref[b, pl.ds(pl.multiple_of(start + 8 * q, 8), 8), :] for q in range(4)
            ]
            parts = list(carry)
            for o in range(24 + tap_count):
                rows = gated_ref[b, pl.ds(start + (HALO - tap_count + 1 + o), 8), :]
                for q in range(4):
                    if 0 <= o - 8 * q < tap_count:
                        parts[o - 8 * q] = parts[o - 8 * q] + grads[q] * rows
            return tuple(parts)

        parts = lax.fori_loop(0, length // 32, taps, (zero,) * tap_count)
        for j in range(tap_count):
            small_ref[b, j : j + 1, :] = jnp.sum(parts[j], axis=0, keepdims=True)
    store.wait()


def gated_kernel(
    later_ref, taps_ref, grad_hbm, value_hbm, gate_hbm, out_value_ref, out_gate_ref,
    ext_ref, value_ref, gate_ref, sems,
):
    length, channels = value_ref.shape
    blocks = channels // LANES
    tap_count = taps_ref.shape[0]
    loads = []
    for b in range(blocks):
        loads.append(
            pltpu.make_async_copy(grad_hbm.at[b], ext_ref.at[b, pl.ds(0, length)], sems.at[b])
        )
    loads.append(pltpu.make_async_copy(value_hbm, value_ref, sems.at[blocks]))
    loads.append(pltpu.make_async_copy(gate_hbm, gate_ref, sems.at[blocks + 1]))
    for load in loads:
        load.start()
    for b in range(blocks):
        ext_ref[b, length : length + HALO, :] = later_ref[b]
    for load in loads:
        load.wait()
    for b in range(blocks):
        lanes = slice(b * LANES, (b + 1) * LANES)

        def conv(i, carry, b=b, lanes=lanes):
            start = pl.multiple_of(i * 64, 64)
            rows = pl.ds(start, 64)
            totals = convolved(
                lambda o: ext_ref[b, pl.ds(start + o, 8), :],
                [
                    jnp.broadcast_to(taps_ref[j : j + 1, lanes], (8, LANES))
                    for j in reversed(range(tap_count))
                ],
                8,
            )
            total = jnp.concatenate(totals, axis=0)
            sig = sigmoid(gate_ref[rows, lanes].astype(F32))
            part = total * sig
            out_value_ref[rows, lanes] = part.astype(BF16)
            out_gate_ref[rows, lanes] = (
                part * value_ref[rows, lanes].astype(F32) * (1.0 - sig)
            ).astype(BF16)
            return carry

        lax.fori_loop(0, length // 64, conv, 0)


def pack_kernel(parts_ref, kept_ref, small_ref, out_ref):
    count = out_ref.shape[0]
    blocks, small_rows, _ = small_ref.shape
    halves = small_rows // 4
    group = lax.axis_index("dp_0")
    weights = [jnp.where(group == x, 0.0, 1.0) for x in range(4)]
    for i in range(count // 4):
        rows = slice(16 * i, 16 * i + 16)
        tiles = []
        for b in range(blocks):
            lanes = slice(b * LANES, (b + 1) * LANES)
            tiles.append(
                kept_ref[rows, lanes]
                + sum(parts_ref[x, rows, lanes].astype(F32) * weights[x] for x in range(4))
            )
        for k in range(2):
            for h in range(2):
                m = 4 * i + 2 * k + h
                pieces = [tiles[2 * h + t][8 * k : 8 * k + 8] for t in range(2)]
                if m < blocks * halves:
                    b, g = m // halves, m % halves
                    tile = small_ref[b, 4 * g : 4 * g + 4, :]
                    high = tile.astype(BF16).astype(F32)
                    pieces += [high, tile - high]
                else:
                    pieces.append(jnp.zeros((8, LANES), F32))
                out_ref[m] = jnp.concatenate(pieces, axis=0).astype(BF16)


def total_kernel(scale, parts_ref, rows_ref, tiles_ref):
    def add(i, carry):
        return carry + parts_ref[i].astype(F32)

    total = lax.fori_loop(
        0, parts_ref.shape[0], add, jnp.zeros(parts_ref.shape[1:], F32), unroll=8
    ) * scale
    rows_ref[...] = total[0:16]
    tile = jnp.concatenate([total[16:20] + total[20:24], jnp.zeros((4, LANES), F32)], axis=0)
    for i in range(tiles_ref.shape[0]):
        tiles_ref[i] = tile


def spread_kernel(rows_ref, tiles_ref, out_ref):
    tile = sum(tiles_ref[i] for i in range(tiles_ref.shape[0]))[0:4]
    high = tile.astype(BF16).astype(F32)
    both = jnp.concatenate([rows_ref[...], high, tile - high], axis=0).astype(BF16)

    def put(i, carry):
        out_ref[i] = both
        return carry

    lax.fori_loop(0, out_ref.shape[0], put, 0, unroll=8)


def unpack_kernel(parts_ref, weight_ref, taps_ref, gain_ref, shift_ref, small_ref):
    count = parts_ref.shape[0]
    small_rows = small_ref.shape[0]
    tap_count = taps_ref.shape[0]
    blocks = small_ref.shape[1] // LANES
    halves = small_rows // 4
    for m in range(count):
        i, h = m // 2, m % 2
        part = parts_ref[m].astype(F32)
        for t in range(2):
            weight_ref[8 * i : 8 * i + 8, (2 * h + t) * LANES : (2 * h + t + 1) * LANES] = part[
                8 * t : 8 * t + 8
            ]
        if m < blocks * halves:
            b, g = m // halves, m % halves
            small_ref[4 * g : 4 * g + 4, b * LANES : (b + 1) * LANES] = part[16:20] + part[20:24]
    taps_ref[...] = small_ref[0:tap_count, :]
    gain_ref[...] = small_ref[tap_count : tap_count + 1, :]
    shift_ref[...] = small_ref[tap_count + 1 : tap_count + 2, :]


def from_behind(value, axis, by):
    count = lax.axis_size(axis)
    pairs = [(i, i + by) for i in range(count) if 0 <= i + by < count]
    return lax.ppermute(value, axis, pairs)


def swapped(value):
    return lax.ppermute(value, "dp_1", [(0, 1), (1, 0)])


def in_hbm(value):
    return pltpu.with_memory_space_constraint(value, pltpu.HBM)


def exchanged(value, axes):
    return lax.all_to_all(value, axes, 0, 0, tiled=True)


def one_device(glu_value, glu_gate, cotangent, conv_weight, norm_gain, norm_shift, out_weight):
    value_rows = glu_value[0]
    gate_rows = glu_gate[0]
    cotan_rows = cotangent[0]
    length, channels = value_rows.shape
    blocks = channels // LANES
    wide = out_weight.shape[0]
    tap_count = conv_weight.shape[0]
    count_sp = lax.axis_size(SP)
    count_dp = lax.axis_size(DP)
    scale = 1.0 / math.sqrt(length * count_sp * count_dp)
    gain = norm_gain.reshape(1, channels)
    shift = norm_shift.reshape(1, channels)
    shaped = jax.ShapeDtypeStruct

    halo, copies = pl.pallas_call(
        prepare_kernel,
        out_shape=(shaped((2 * HALO, channels), BF16), shaped((4, wide, channels), BF16)),
        in_specs=[HBM] * 3,
        out_specs=(VMEM, HBM),
        scratch_shapes=[pltpu.VMEM((wide, channels), BF16), pltpu.SemaphoreType.DMA((7,))],
        compiler_params=params(62),
        cost_estimate=cost(1),
        name="prepare",
    )(value_rows, gate_rows, out_weight)
    halo = from_behind(halo, SP, 1)
    other_cotan = swapped(cotan_rows)
    own_weight = exchanged(copies, "dp_0")

    act, normed, inv = pl.pallas_call(
        forward_kernel,
        out_shape=(
            shaped((length, channels), BF16),
            pltpu.HBM((blocks, length, LANES), F32),
            pltpu.HBM((length, LANES), F32),
        ),
        in_specs=[VMEM] * 6,
        out_specs=(VMEM, HBM, HBM),
        scratch_shapes=[
            pltpu.VMEM((blocks, length, LANES), F32),
            pltpu.VMEM((length, LANES), F32),
            pltpu.VMEM((blocks, length + HALO, LANES), F32),
            pltpu.SemaphoreType.DMA((2, length // 64)),
        ],
        compiler_params=params(8),
        cost_estimate=cost(6),
        name="module_forward",
    )(conv_weight, gain, shift, halo, value_rows, gate_rows)
    other_act = swapped(act)
    sent, kept = pl.pallas_call(
        weight_kernel,
        out_shape=(pltpu.HBM((4, wide, channels), BF16), pltpu.HBM((wide, channels), F32)),
        in_specs=[VMEM] * 4,
        out_specs=(HBM,) * 2,
        scratch_shapes=[
            pltpu.VMEM((4, wide, channels), BF16),
            pltpu.VMEM((wide, channels), F32),
            pltpu.SemaphoreType.DMA((5,)),
        ],
        compiler_params=params(8),
        cost_estimate=cost(3),
        name="weight_term",
    )(act, other_act, cotan_rows, other_cotan)
    own_weight, kept = lax.optimization_barrier((own_weight, kept))
    other_weight = swapped(own_weight)
    arrived = exchanged(sent, "dp_0")

    small_rows = -(-(tap_count + 2) // 8) * 8
    grad, head, small = pl.pallas_call(
        backward_kernel,
        out_shape=(
            pltpu.HBM((blocks, length, LANES), F32),
            shaped((blocks, HALO, LANES), F32),
            shaped((blocks, small_rows, LANES), F32),
        ),
        in_specs=[HBM] * 8 + [VMEM, HBM],
        out_specs=(HBM, VMEM, VMEM),
        scratch_shapes=[
            pltpu.VMEM((1, channels), F32),
            pltpu.VMEM((1, channels), F32),
            pltpu.VMEM((blocks, length, LANES), F32),
            pltpu.VMEM((length, LANES), F32),
            pltpu.VMEM((2 * HALO, channels), BF16),
            pltpu.VMEM((length, channels), BF16),
            pltpu.VMEM((length, channels), BF16),
            pltpu.VMEM((4, wide, channels), BF16),
            pltpu.VMEM((8, length, wide), BF16),
            pltpu.VMEM((blocks, length, LANES), F32),
            pltpu.VMEM((blocks, length + HALO, LANES), F32),
            pltpu.SemaphoreType.DMA((8,)),
            pltpu.SemaphoreType.DMA((8,)),
            pltpu.SemaphoreType.DMA,
        ],
        compiler_params=params(14),
        cost_estimate=cost(10),
        name="module_backward",
    )(
        *(in_hbm(a) for a in (gain, shift, normed, inv, halo, value_rows, gate_rows)),
        in_hbm(own_weight), other_weight, in_hbm(cotan_rows),
    )
    later = from_behind(head, SP, -1)

    packed = pl.pallas_call(
        pack_kernel,
        out_shape=shaped((count_sp, 24, LANES), BF16),
        in_specs=[VMEM] * 3,
        out_specs=VMEM,
        compiler_params=params(8),
        cost_estimate=cost(1),
        name="pack",
    )(arrived, kept, small)
    grad_value, grad_gate = pl.pallas_call(
        gated_kernel,
        out_shape=(shaped((length, channels), BF16), shaped((length, channels), BF16)),
        in_specs=[VMEM] * 2 + [HBM] * 3,
        out_specs=(VMEM,) * 2,
        scratch_shapes=[
            pltpu.VMEM((blocks, length + HALO, LANES), F32),
            pltpu.VMEM((length, channels), BF16),
            pltpu.VMEM((length, channels), BF16),
            pltpu.SemaphoreType.DMA((blocks + 2,)),
        ],
        compiler_params=params(62),
        cost_estimate=cost(6),
        name="gated_backward",
    )(later, conv_weight, grad, value_rows, gate_rows)

    terms = exchanged(packed, SP)
    rows, tiles = pl.pallas_call(
        functools.partial(total_kernel, scale),
        out_shape=(shaped((16, LANES), F32), shaped((count_dp, 8, LANES), F32)),
        in_specs=[VMEM],
        out_specs=(VMEM,) * 2,
        compiler_params=params(4),
        cost_estimate=cost(1),
        name="total",
    )(terms)
    tiles = exchanged(tiles, DP)
    totals = pl.pallas_call(
        spread_kernel,
        out_shape=shaped((count_sp, 24, LANES), BF16),
        in_specs=[VMEM] * 2,
        out_specs=VMEM,
        compiler_params=params(4),
        cost_estimate=cost(1),
        name="spread",
    )(rows, tiles)
    whole = exchanged(totals, SP)
    grad_out_weight, grad_conv, grad_gain, grad_shift = pl.pallas_call(
        unpack_kernel,
        out_shape=(
            shaped((wide, channels), F32),
            shaped((tap_count, channels), F32),
            shaped((1, channels), F32),
            shaped((1, channels), F32),
        ),
        in_specs=[VMEM],
        out_specs=(VMEM,) * 4,
        scratch_shapes=[pltpu.VMEM((small_rows, channels), F32)],
        compiler_params=params(8),
        cost_estimate=cost(1),
        name="unpack",
    )(whole)
    return (
        grad_value[None],
        grad_gate[None],
        grad_out_weight,
        grad_conv,
        grad_gain.reshape(channels),
        grad_shift.reshape(channels),
    )


def solution(mesh):
    split = Mesh(mesh.devices.reshape(8, 8, 4, 2), ("sp_0", "sp_1", "dp_0", "dp_1"))
    return jax.shard_map(
        one_device,
        mesh=split,
        in_specs=(P(DP, SP, None), P(DP, SP, None), P(DP, SP, None), P(), P(), P(), P(DP, None)),
        out_specs=(P(DP, SP, None), P(DP, SP, None), P(DP, None), P(), P(), P()),
        check_vma=False,
    )
```

time: 127 us -> 117 us (0.921)
  Pallas kernels: 34.4 us -> 29.8 us
  local copies, waits for them, and re-layouts: 5.11 us -> 0.68 us
  waiting for transfers between devices: 16.8 us -> 18.4 us
    ppermute x2, waiting for transfers between devices: 1.7 us -> 8.98 us  [from_behind(): return lax.ppermute(value, axis, pairs)]
    all_to_all x3, waiting for transfers between devices: 13.7 us -> 7.57 us  [exchanged(): return lax.all_to_all(value, axes, 0, 0, tiled=True)]
    pallas_call x8 -> x9, Pallas kernels: 34.4 us -> 29.8 us  [the longest x1 9.62 us: one_device(): pl.pallas_call(backward_kernel, out_shape=(pltpu.HBM((blocks, length, LAN...]
    broadcast_in_dim x1 -> x0, local copies, waits for them, and re-layouts: 2 us -> none  [per_device(): jnp.broadcast_to(out_weight[None], (4, *out_weight.shape))]
    unnamed x12 -> x18, local copies, waits for them, and re-layouts: 2.32 us -> 0.68 us
  transfers between devices with their start and end apart: 8 -> 8, of which waited for: 5 -> 4; matrix products, arithmetic and copies ran while one was open for 3% -> 0% of each run, Pallas kernels for 26% -> 24%
where the time goes in v2:
time: 117 us; the launch traced here: 116 us
  blocking collectives  37.2 us (32%)
  Pallas kernels  29.8 us (25%)
  starting transfers between devices  28.6 us (24%)
  waiting for transfers between devices  18.4 us (16%)
    all_to_all x2, blocking collectives, exchanged(): return lax.all_to_all(value, axes, 0, 0, tiled=True)  37.2 us
    ppermute x3, starting transfers between devices, swapped(): return lax.ppermute(value, 'dp_1', [(0, 1), (1, 0)])  13.6 us
    all_to_all x3, starting transfers between devices, exchanged(): return lax.all_to_all(value, axes, 0, 0, tiled=True)  12.4 us
    pallas_call x1, Pallas kernels, one_device(): pl.pallas_call(backward_kernel, out_shape=(pltpu.HBM((blocks, length, LAN...  9.62 us
    ppermute x2, waiting for transfers between devices, from_behind(): return lax.ppermute(value, axis, pairs)  8.98 us
    all_to_all x3, waiting for transfers between devices, exchanged(): return lax.all_to_all(value, axes, 0, 0, tiled=True)  7.57 us
    pallas_call x1, Pallas kernels, one_device(): pl.pallas_call(gated_kernel, out_shape=(shaped((length, channels), BF16),...  6.31 us
    pallas_call x1, Pallas kernels, one_device(): pl.pallas_call(forward_kernel, out_shape=(shaped((length, channels), BF16...  5.54 us
  transfers between devices with their start and end apart: 8, of which 4 were waited for; matrix products, arithmetic and copies ran while one was open for 0% of the time, Pallas kernels for 24%

profile of v2, /device:TPU:1, one launch (start us, length us, event | category | flops | bytes accessed | tf_op | source)
XLA Modules:
  0.0 115.5 jit_solution(16729391711049400671)
XLA Ops:
  0.6 0.0 copy-start.3
  0.6 0.0 copy-start.2
  0.7 0.0 copy-start.4
  0.7 0.0 copy-start.7
  0.7 0.0 copy-start.6
  0.7 8.9 %collective-permute-start.2 = (bf16[512,2048]{1,0:T(8,128)(2,1)}, bf16[512,2048]{1,0:T(8,128)(2,1)}, u32[]{:S(2)}, u32[]{:S(2)}) collective-permute-start(bf16[512,2048]{1,0:T(8,128)(2,1)} %bitcast.9), channel_id=1, source_target_pairs={{0,1},{1,0},{2,3},{3,2},{4,5},{5,4},{6,7},{7,6},{8,9},{9,8},{10,11... | collective-permute-start | bytes 6291464 | tf_op jit(solution)/shard_map/ppermute | solution.py:426
  9.6 2.6 %prepare.1 = (bf16[64,512]{1,0:T(8,128)(2,1)}, bf16[4,256,512]{2,1,0:T(8,128)(2,1)}) custom-call(bf16[512,512]{1,0:T(8,128)(2,1)} %bitcast.12, bf16[512,512]{1,0:T(8,128)(2,1)} %bitcast.16, bf16[256,512]{1,0:T(8,128)(2,1)} %weight_hbm.1), custom_call_target="tpu_custom_call" | custom-call | flops 500000000 | bytes 1048576 | tf_op jit(solution)/shard_map/prepare/pallas_call | solution.py:452
  12.2 1.3 %collective-permute-start = (bf16[64,512]{1,0:T(8,128)(2,1)}, bf16[64,512]{1,0:T(8,128)(2,1)S(1)}, u32[]{:S(2)}, u32[]{:S(2)}) collective-permute-start(bf16[64,512]{1,0:T(8,128)(2,1)} %get-tuple-element.26), channel_id=1, source_target_pairs={{0,8},{8,16},{16,24},{24,32},{32,40},{40,48},{48,56},{56,64},{64,7... | collective-permute-start | bytes 196616 | tf_op jit(solution)/shard_map/ppermute | solution.py:422
  13.5 4.3 %all-to-all-start = ((bf16[4,256,512]{2,1,0:T(8,128)(2,1)}), bf16[4,256,512]{2,1,0:T(8,128)(2,1)}, u32[]{:S(2)}, u32[]{:S(2)}) async-start(bf16[4,256,512]{2,1,0:T(8,128)(2,1)} %get-tuple-element.29), calls=%async_computation | async-start | bytes 2097152 | tf_op jit(solution)/shard_map/all_to_all | solution.py:434
  17.8 0.0 collective-permute-done.halo_ref.halo_hbm
  17.8 0.0 copy-start.5
  17.8 0.0 copy-done.3
  17.8 0.0 copy-done.2
  17.8 0.0 copy-done.4
  17.8 0.0 copy-done.7
  17.8 0.0 copy-done.6
  17.9 0.0 copy-start.1
  17.9 5.5 %module_forward.1 = (bf16[512,512]{1,0:T(8,128)(2,1)S(1)}, f32[4,512,128]{2,1,0:T(8,128)}, f32[512,128]{1,0:T(8,128)}) custom-call(f32[31,512]{1,0:T(8,128)S(1)} %copy-done.4, f32[1,512]{1,0:T(1,128)S(1)} %bitcast.21, f32[1,512]{1,0:T(1,128)S(1)} %bitcast.23, bf16[64,512]{1,0:T(8,128)(2,1)S(1)} %collective-permute-done.halo_ref.halo_hbm, ...), custom_call_target="tpu_custom_call" | custom-call | flops 3000000000 | bytes 1048576 | tf_op jit(solution)/shard_map/module_forward/pallas_call | solution.py:466
  23.4 0.0 copy-done.5
  23.4 1.9 %collective-permute-start.1 = (bf16[512,512]{1,0:T(8,128)(2,1)S(1)}, bf16[512,512]{1,0:T(8,128)(2,1)S(1)}, u32[]{:S(2)}, u32[]{:S(2)}) collective-permute-start(bf16[512,512]{1,0:T(8,128)(2,1)S(1)} %get-tuple-element.30.act_ref), channel_id=1, source_target_pairs={{0,1},{1,0},{2,3},{3,2},{4,5},{5,4},{6,7},{7,6},{8,9},{9,8},{10,11... | collective-permute-start | bytes 1572872 | tf_op jit(solution)/shard_map/ppermute | solution.py:426
  25.4 1.9 %collective-permute-done.1.other_act_ref = bf16[512,512]{1,0:T(8,128)(2,1)S(1)} collective-permute-done((bf16[512,512]{1,0:T(8,128)(2,1)S(1)}, bf16[512,512]{1,0:T(8,128)(2,1)S(1)}, u32[]{:S(2)}, u32[]{:S(2)}) %collective-permute-start.1) | collective-permute-done | bytes 524320 | tf_op jit(solution)/shard_map/ppermute | solution.py:426
  27.2 0.0 collective-permute-done.2.other_cotan_ref
  27.2 0.0 copy-done.1
  27.2 3.7 %weight_term.1 = (bf16[4,256,512]{2,1,0:T(8,128)(2,1)}, f32[256,512]{1,0:T(8,128)}) custom-call(bf16[512,512]{1,0:T(8,128)(2,1)S(1)} %get-tuple-element.30.act_ref, bf16[512,512]{1,0:T(8,128)(2,1)S(1)} %collective-permute-done.1.other_act_ref, bf16[512,2048]{1,0:T(8,128)(2,1)S(1)} %bitcast.11, bf16[512,2048]{1,0:T(8,128)(2,1)} %collective-permute-done.2.other_cotan_ref), custom_call_target="tpu_custom_call" | custom-call | flops 1500000000 | bytes 1048576 | tf_op jit(solution)/shard_map/weight_term/pallas_call | solution.py:486
  30.9 2.1 %all-to-all-done.own_hbm = bf16[4,256,512]{2,1,0:T(8,128)(2,1)} async-done(((bf16[4,256,512]{2,1,0:T(8,128)(2,1)}), bf16[4,256,512]{2,1,0:T(8,128)(2,1)}, u32[]{:S(2)}, u32[]{:S(2)}) %all-to-all-start) | async-done | bytes 1048608 | tf_op jit(solution)/shard_map/all_to_all | solution.py:434
  33.0 2.8 %collective-permute-start.3 = (bf16[4,256,512]{2,1,0:T(8,128)(2,1)}, bf16[4,256,512]{2,1,0:T(8,128)(2,1)S(1)}, u32[]{:S(2)}, u32[]{:S(2)}) collective-permute-start(bf16[4,256,512]{2,1,0:T(8,128)(2,1)} %all-to-all-done.own_hbm), channel_id=1, source_target_pairs={{0,1},{1,0},{2,3},{3,2},{4,5},{5,4},{6,7},{7,6},{8,9},{9,8},{10,11... | collective-permute-start | bytes 3145736 | tf_op jit(solution)/shard_map/ppermute | solution.py:426
  35.8 3.5 %all-to-all-start.1 = ((bf16[4,256,512]{2,1,0:T(8,128)(2,1)}), bf16[4,256,512]{2,1,0:T(8,128)(2,1)S(1)}, u32[]{:S(2)}, u32[]{:S(2)}) async-start(bf16[4,256,512]{2,1,0:T(8,128)(2,1)} %get-tuple-element.37), calls=%async_computation.1 | async-start | bytes 2097152 | tf_op jit(solution)/shard_map/all_to_all | solution.py:434
  39.3 0.0 collective-permute-done.3.other_ref
  39.3 0.0 copy-start
  39.4 9.6 %module_backward.1 = (f32[4,512,128]{2,1,0:T(8,128)}, f32[4,32,128]{2,1,0:T(8,128)S(1)}, f32[4,40,128]{2,1,0:T(8,128)S(1)}) custom-call(f32[1,512]{1,0:T(1,128)} %bitcast.20, f32[1,512]{1,0:T(1,128)} %bitcast.22, f32[4,512,128]{2,1,0:T(8,128)} %get-tuple-element.27.normed_hbm, f32[512,128]{1,0:T(8,128)} %get-tuple-element.28.inv_hbm, ...), custom_call_target="tpu_custom_call" | custom-call | flops 5000000000 | bytes 1048576 | tf_op jit(solution)/shard_map/module_backward/pallas_call | solution.py:505
  49.0 5.5 %all-to-all-done.1.parts_ref = bf16[4,256,512]{2,1,0:T(8,128)(2,1)S(1)} async-done(((bf16[4,256,512]{2,1,0:T(8,128)(2,1)}), bf16[4,256,512]{2,1,0:T(8,128)(2,1)S(1)}, u32[]{:S(2)}, u32[]{:S(2)}) %all-to-all-start.1) | async-done | bytes 1048608 | tf_op jit(solution)/shard_map/all_to_all | solution.py:434
  54.5 0.0 copy-done
  54.5 0.3 pack.1
  54.7 26.5 %all_to_all.25.parts_ref = bf16[64,24,128]{2,1,0:T(8,128)(2,1)S(1)} all-to-all(bf16[64,24,128]{2,1,0:T(8,128)(2,1)S(1)} %pack.1), channel_id=1, replica_groups=mesh['sp_0'=8,'sp_1'=8,'dp_0'=4,'dp_1'=2] {'sp_0','sp_1'}, dimensions={0} | all-to-all | bytes 786432 | tf_op jit(solution)/shard_map/all_to_all | solution.py:434
  81.2 0.1 total.1
  81.3 10.7 %all_to_all.26.tiles_ref = f32[8,8,128]{2,1,0:T(8,128)S(1)} all-to-all(f32[8,8,128]{2,1,0:T(8,128)S(1)} %get-tuple-element.41), channel_id=1, replica_groups=mesh['sp_0'=8,'sp_1'=8,'dp_0'=4,'dp_1'=2] {'dp_0','dp_1'}, dimensions={0} | all-to-all | bytes 65536 | tf_op jit(solution)/shard_map/all_to_all | solution.py:434
  92.0 0.8 spread.1
  92.8 4.6 %all-to-all-start.4 = ((bf16[64,24,128]{2,1,0:T(8,128)(2,1)}), bf16[64,24,128]{2,1,0:T(8,128)(2,1)S(1)}, u32[]{:S(2)}, u32[]{:S(2)}) async-start(bf16[64,24,128]{2,1,0:T(8,128)(2,1)} %spread.1), calls=%async_computation.4 | async-start | bytes 786432 | tf_op jit(solution)/shard_map/all_to_all | solution.py:434
  97.4 1.3 %collective-permute-start.4 = (f32[4,32,128]{2,1,0:T(8,128)S(1)}, f32[4,32,128]{2,1,0:T(8,128)S(1)}, u32[]{:S(2)}, u32[]{:S(2)}) collective-permute-start(f32[4,32,128]{2,1,0:T(8,128)S(1)} %get-tuple-element.33), channel_id=1, source_target_pairs={{8,0},{16,8},{24,16},{32,24},{40,32},{48,40},{56,48},{64,56},{72,6... | collective-permute-start | bytes 196616 | tf_op jit(solution)/shard_map/ppermute | solution.py:422
  98.7 9.0 %collective-permute-done.4.later_ref = f32[4,32,128]{2,1,0:T(8,128)S(1)} collective-permute-done((f32[4,32,128]{2,1,0:T(8,128)S(1)}, f32[4,32,128]{2,1,0:T(8,128)S(1)}, u32[]{:S(2)}, u32[]{:S(2)}) %collective-permute-start.4) | collective-permute-done | bytes 65568 | tf_op jit(solution)/shard_map/ppermute | solution.py:422
  107.7 0.0 copy-start.8
  107.7 0.6 copy-done.8
  108.3 6.3 %gated_backward.1 = (bf16[512,512]{1,0:T(8,128)(2,1)}, bf16[512,512]{1,0:T(8,128)(2,1)}) custom-call(f32[4,32,128]{2,1,0:T(8,128)} %copy-done.8, f32[31,512]{1,0:T(8,128)} %taps_ref.3, f32[4,512,128]{2,1,0:T(8,128)} %get-tuple-element.34.grad_hbm, bf16[512,512]{1,0:T(8,128)(2,1)} %bitcast.14, bf16[512,512]{1,0:T(8,128)(2,1)} %bitcast.18), custom_call_target="tpu_custom_call" | custom-call | flops 3000000000 | bytes 1048576 | tf_op jit(solution)/shard_map/gated_backward/pallas_call | solution.py:548
  114.7 0.0 all-to-all-done.4.parts_ref
  114.7 0.9 unpack.1
Async XLA Ops:
  0.6 17.2 %copy-start.3 = (bf16[1,512,512]{2,1,0:T(8,128)(2,1)S(1)}, bf16[1,512,512]{2,1,0:T(8,128)(2,1)}, u32[]{:S(2)}) copy-start(bf16[1,512,512]{2,1,0:T(8,128)(2,1)} %param.8) | copy-start | bytes 1572868
  0.6 17.2 %copy-start.2 = (bf16[1,512,512]{2,1,0:T(8,128)(2,1)S(1)}, bf16[1,512,512]{2,1,0:T(8,128)(2,1)}, u32[]{:S(2)}) copy-start(bf16[1,512,512]{2,1,0:T(8,128)(2,1)} %param.7) | copy-start | bytes 1572868
  0.7 17.2 %copy-start.4 = (f32[31,512]{1,0:T(8,128)S(1)}, f32[31,512]{1,0:T(8,128)}, u32[]{:S(2)}) copy-start(f32[31,512]{1,0:T(8,128)} %taps_ref.3) | copy-start | bytes 190468
  0.7 17.2 %copy-start.7 = (f32[512]{0:T(512)S(1)}, f32[512]{0:T(512)}, u32[]{:S(2)}) copy-start(f32[512]{0:T(512)} %param.12) | copy-start | bytes 6148
  0.7 17.2 %copy-start.6 = (f32[512]{0:T(512)S(1)}, f32[512]{0:T(512)}, u32[]{:S(2)}) copy-start(f32[512]{0:T(512)} %param.11) | copy-start | bytes 6148
  0.7 26.5 %collective-permute-start.2 = (bf16[512,2048]{1,0:T(8,128)(2,1)}, bf16[512,2048]{1,0:T(8,128)(2,1)}, u32[]{:S(2)}, u32[]{:S(2)}) collective-permute-start(bf16[512,2048]{1,0:T(8,128)(2,1)} %bitcast.9), channel_id=1, source_target_pairs={{0,1},{1,0},{2,3},{3,2},{4,5},{5,4},{6,7},{7,6},{8,9},{9,8},{10,11... | collective-permute-start | bytes 6291464 | tf_op jit(solution)/shard_map/ppermute | solution.py:426
  12.2 5.6 %collective-permute-start = (bf16[64,512]{1,0:T(8,128)(2,1)}, bf16[64,512]{1,0:T(8,128)(2,1)S(1)}, u32[]{:S(2)}, u32[]{:S(2)}) collective-permute-start(bf16[64,512]{1,0:T(8,128)(2,1)} %get-tuple-element.26), channel_id=1, source_target_pairs={{0,8},{8,16},{16,24},{24,32},{32,40},{40,48},{48,56},{56,64},{64,7... | collective-permute-start | bytes 196616 | tf_op jit(solution)/shard_map/ppermute | solution.py:422
  13.5 19.5 %all-to-all-start = ((bf16[4,256,512]{2,1,0:T(8,128)(2,1)}), bf16[4,256,512]{2,1,0:T(8,128)(2,1)}, u32[]{:S(2)}, u32[]{:S(2)}) async-start(bf16[4,256,512]{2,1,0:T(8,128)(2,1)} %get-tuple-element.29), calls=%async_computation | async-start | bytes 2097152 | tf_op jit(solution)/shard_map/all_to_all | solution.py:434
  17.8 5.6 %copy-start.5 = (bf16[64,512]{1,0:T(8,128)(2,1)}, bf16[64,512]{1,0:T(8,128)(2,1)S(1)}, u32[]{:S(2)}) copy-start(bf16[64,512]{1,0:T(8,128)(2,1)S(1)} %collective-permute-done.halo_ref.halo_hbm) | copy-start | bytes 196612
  17.9 9.4 %copy-start.1 = (bf16[1,512,2048]{2,1,0:T(8,128)(2,1)S(1)}, bf16[1,512,2048]{2,1,0:T(8,128)(2,1)}, u32[]{:S(2)}) copy-start(bf16[1,512,2048]{2,1,0:T(8,128)(2,1)} %param.9) | copy-start | bytes 6291460
  23.4 3.8 %collective-permute-start.1 = (bf16[512,512]{1,0:T(8,128)(2,1)S(1)}, bf16[512,512]{1,0:T(8,128)(2,1)S(1)}, u32[]{:S(2)}, u32[]{:S(2)}) collective-permute-start(bf16[512,512]{1,0:T(8,128)(2,1)S(1)} %get-tuple-element.30.act_ref), channel_id=1, source_target_pairs={{0,1},{1,0},{2,3},{3,2},{4,5},{5,4},{6,7},{7,6},{8,9},{9,8},{10,11... | collective-permute-start | bytes 1572872 | tf_op jit(solution)/shard_map/ppermute | solution.py:426
  33.0 6.3 %collective-permute-start.3 = (bf16[4,256,512]{2,1,0:T(8,128)(2,1)}, bf16[4,256,512]{2,1,0:T(8,128)(2,1)S(1)}, u32[]{:S(2)}, u32[]{:S(2)}) collective-permute-start(bf16[4,256,512]{2,1,0:T(8,128)(2,1)} %all-to-all-done.own_hbm), channel_id=1, source_target_pairs={{0,1},{1,0},{2,3},{3,2},{4,5},{5,4},{6,7},{7,6},{8,9},{9,8},{10,11... | collective-permute-start | bytes 3145736 | tf_op jit(solution)/shard_map/ppermute | solution.py:426
  35.8 18.7 %all-to-all-start.1 = ((bf16[4,256,512]{2,1,0:T(8,128)(2,1)}), bf16[4,256,512]{2,1,0:T(8,128)(2,1)S(1)}, u32[]{:S(2)}, u32[]{:S(2)}) async-start(bf16[4,256,512]{2,1,0:T(8,128)(2,1)} %get-tuple-element.37), calls=%async_computation.1 | async-start | bytes 2097152 | tf_op jit(solution)/shard_map/all_to_all | solution.py:434
  39.3 15.1 %copy-start = (f32[256,512]{1,0:T(8,128)S(1)}, f32[256,512]{1,0:T(8,128)}, u32[]{:S(2)}) copy-start(f32[256,512]{1,0:T(8,128)} %get-tuple-element.38.kept_ref) | copy-start | bytes 1572868
  92.8 21.9 %all-to-all-start.4 = ((bf16[64,24,128]{2,1,0:T(8,128)(2,1)}), bf16[64,24,128]{2,1,0:T(8,128)(2,1)S(1)}, u32[]{:S(2)}, u32[]{:S(2)}) async-start(bf16[64,24,128]{2,1,0:T(8,128)(2,1)} %spread.1), calls=%async_computation.4 | async-start | bytes 786432 | tf_op jit(solution)/shard_map/all_to_all | solution.py:434
  97.4 10.3 %collective-permute-start.4 = (f32[4,32,128]{2,1,0:T(8,128)S(1)}, f32[4,32,128]{2,1,0:T(8,128)S(1)}, u32[]{:S(2)}, u32[]{:S(2)}) collective-permute-start(f32[4,32,128]{2,1,0:T(8,128)S(1)} %get-tuple-element.33), channel_id=1, source_target_pairs={{8,0},{16,8},{24,16},{32,24},{40,32},{48,40},{56,48},{64,56},{72,6... | collective-permute-start | bytes 196616 | tf_op jit(solution)/shard_map/ppermute | solution.py:422
  107.7 0.6 copy-start.8

commit v3 on v2

--- a/solution.py
+++ b/solution.py
@@ -75,7 +75,7 @@
     length, channels = value_ref.shape
     blocks = channels // LANES
     tap_count = taps_ref.shape[0]
-    step = 64
+    step = 128
     steps = length // step
 
     def row_stores(i):
@@ -175,7 +175,7 @@
     me = lax.axis_index("dp_1")
     wide = own_ref.shape[1]
     tap_count = 31
-    step = 128
+    step = 512
     columns = [
         pltpu.make_async_copy(
             cotan_hbm.at[:, pl.ds(pl.multiple_of((2 * x + parity) * wide, wide), wide)],
@@ -240,7 +240,7 @@
         load.wait()
 
     def point(i, carry):
-        rows = pl.ds(pl.multiple_of(i * 32, 32), 32)
+        rows = pl.ds(pl.multiple_of(i * 128, 128), 128)
         inv = inv_ref[rows, :]
         grads = []
         normeds = []
@@ -252,8 +252,8 @@
             pre = normed * gain_ref[:, lanes] + shift_ref[:, lanes]
             sig = sigmoid(pre)
             grad_pre = grad_ref[b, rows, :] * (sig + pre * sig * (1.0 - sig))
-            gains.append(carry[b] + jnp.sum((grad_pre * normed).reshape(4, 8, LANES), axis=0))
-            shifts.append(carry[blocks + b] + jnp.sum(grad_pre.reshape(4, 8, LANES), axis=0))
+            gains.append(carry[b] + jnp.sum((grad_pre * normed).reshape(16, 8, LANES), axis=0))
+            shifts.append(carry[blocks + b] + jnp.sum(grad_pre.reshape(16, 8, LANES), axis=0))
             grads.append(grad_pre * gain_ref[:, lanes])
             normeds.append(normed)
         first = jnp.sum(sum(grads), axis=-1, keepdims=True) / channels
@@ -265,7 +265,7 @@
         return tuple(gains + shifts)
 
     zero = jnp.zeros((8, LANES), F32)
-    sums = lax.fori_loop(0, length // 32, point, (zero,) * (2 * blocks))
+    sums = lax.fori_loop(0, length // 128, point, (zero,) * (2 * blocks))
     store = pltpu.make_async_copy(grad_ref, grad_hbm, out_sem)
     store.start()
     for b in range(blocks):
@@ -277,19 +277,19 @@
         )
 
         def taps(i, carry, b=b):
-            start = pl.multiple_of(i * 32, 32)
+            start = pl.multiple_of(i * 64, 64)
             grads = [
-                grad_ref[b, pl.ds(pl.multiple_of(start + 8 * q, 8), 8), :] for q in range(4)
+                grad_ref[b, pl.ds(pl.multiple_of(start + 8 * q, 8), 8), :] for q in range(8)
             ]
             parts = list(carry)
-            for o in range(24 + tap_count):
+            for o in range(56 + tap_count):
                 rows = gated_ref[b, pl.ds(start + (HALO - tap_count + 1 + o), 8), :]
-                for q in range(4):
+                for q in range(8):
                     if 0 <= o - 8 * q < tap_count:
                         parts[o - 8 * q] = parts[o - 8 * q] + grads[q] * rows
             return tuple(parts)
 
-        parts = lax.fori_loop(0, length // 32, taps, (zero,) * tap_count)
+        parts = lax.fori_loop(0, length // 64, taps, (zero,) * tap_count)
         for j in range(tap_count):
             small_ref[b, j : j + 1, :] = jnp.sum(parts[j], axis=0, keepdims=True)
     store.wait()
@@ -319,15 +319,15 @@
         lanes = slice(b * LANES, (b + 1) * LANES)
 
         def conv(i, carry, b=b, lanes=lanes):
-            start = pl.multiple_of(i * 64, 64)
-            rows = pl.ds(start, 64)
+            start = pl.multiple_of(i * 128, 128)
+            rows = pl.ds(start, 128)
             totals = convolved(
                 lambda o: ext_ref[b, pl.ds(start + o, 8), :],
                 [
                     jnp.broadcast_to(taps_ref[j : j + 1, lanes], (8, LANES))
                     for j in reversed(range(tap_count))
                 ],
-                8,
+                16,
             )
             total = jnp.concatenate(totals, axis=0)
             sig = sigmoid(gate_ref[rows, lanes].astype(F32))
@@ -338,7 +338,7 @@
             ).astype(BF16)
             return carry
 
-        lax.fori_loop(0, length // 64, conv, 0)
+        lax.fori_loop(0, length // 128, conv, 0)
 
 
 def pack_kernel(parts_ref, kept_ref, small_ref, out_ref):
@@ -476,7 +476,7 @@
             pltpu.VMEM((blocks, length, LANES), F32),
             pltpu.VMEM((length, LANES), F32),
             pltpu.VMEM((blocks, length + HALO, LANES), F32),
-            pltpu.SemaphoreType.DMA((2, length // 64)),
+            pltpu.SemaphoreType.DMA((2, length // 128)),
         ],
         compiler_params=params(8),
         cost_estimate=cost(6),

time: 117 us -> 117 us (level)
  Pallas kernels: 29.8 us -> 26.2 us
  waiting for transfers between devices: 18.4 us -> 21.7 us
    all_to_all x3, waiting for transfers between devices: 7.57 us -> 10.8 us  [exchanged(): return lax.all_to_all(value, axes, 0, 0, tiled=True)]
    pallas_call x1, Pallas kernels: 9.62 us -> 7.13 us  [one_device(): pl.pallas_call(backward_kernel, out_shape=(pltpu.HBM((blocks, length, LAN...]
  transfers between devices with their start and end apart: 8 -> 8, of which waited for: 4 -> 4; matrix products, arithmetic and copies ran while one was open for 0% -> 0% of each run, Pallas kernels for 24% -> 21%
where the time goes in v3:
time: 117 us; the launch traced here: 115 us
  blocking collectives  37.2 us (32%)
  starting transfers between devices  28.6 us (24%)
  Pallas kernels  26.2 us (22%)
  waiting for transfers between devices  21.7 us (19%)
    all_to_all x2, blocking collectives, exchanged(): return lax.all_to_all(value, axes, 0, 0, tiled=True)  37.2 us
    ppermute x3, starting transfers between devices, swapped(): return lax.ppermute(value, 'dp_1', [(0, 1), (1, 0)])  13.6 us
    all_to_all x3, starting transfers between devices, exchanged(): return lax.all_to_all(value, axes, 0, 0, tiled=True)  12.4 us
    all_to_all x3, waiting for transfers between devices, exchanged(): return lax.all_to_all(value, axes, 0, 0, tiled=True)  10.8 us
    ppermute x2, waiting for transfers between devices, from_behind(): return lax.ppermute(value, axis, pairs)  8.98 us
    pallas_call x1, Pallas kernels, one_device(): pl.pallas_call(backward_kernel, out_shape=(pltpu.HBM((blocks, length, LAN...  7.13 us
    pallas_call x1, Pallas kernels, one_device(): pl.pallas_call(gated_kernel, out_shape=(shaped((length, channels), BF16),...  6 us
    pallas_call x1, Pallas kernels, one_device(): pl.pallas_call(forward_kernel, out_shape=(shaped((length, channels), BF16...  4.76 us
  transfers between devices with their start and end apart: 8, of which 4 were waited for; matrix products, arithmetic and copies ran while one was open for 0% of the time, Pallas kernels for 21%

profile of v3, /device:TPU:1, one launch (start us, length us, event | category | flops | bytes accessed | tf_op | source)
XLA Modules:
  0.0 115.2 jit_solution(12862151517903562979)
XLA Ops:
  0.6 0.0 copy-start.3
  0.6 0.0 copy-start.2
  0.7 0.0 copy-start.4
  0.7 0.0 copy-start.7
  0.7 0.0 copy-start.6
  0.7 8.9 %collective-permute-start.2 = (bf16[512,2048]{1,0:T(8,128)(2,1)}, bf16[512,2048]{1,0:T(8,128)(2,1)}, u32[]{:S(2)}, u32[]{:S(2)}) collective-permute-start(bf16[512,2048]{1,0:T(8,128)(2,1)} %bitcast.9), channel_id=1, source_target_pairs={{0,1},{1,0},{2,3},{3,2},{4,5},{5,4},{6,7},{7,6},{8,9},{9,8},{10,11... | collective-permute-start | bytes 6291464 | tf_op jit(solution)/shard_map/ppermute | solution.py:426
  9.6 2.6 %prepare.1 = (bf16[64,512]{1,0:T(8,128)(2,1)}, bf16[4,256,512]{2,1,0:T(8,128)(2,1)}) custom-call(bf16[512,512]{1,0:T(8,128)(2,1)} %bitcast.12, bf16[512,512]{1,0:T(8,128)(2,1)} %bitcast.16, bf16[256,512]{1,0:T(8,128)(2,1)} %weight_hbm.1), custom_call_target="tpu_custom_call" | custom-call | flops 500000000 | bytes 1048576 | tf_op jit(solution)/shard_map/prepare/pallas_call | solution.py:452
  12.2 1.3 %collective-permute-start = (bf16[64,512]{1,0:T(8,128)(2,1)}, bf16[64,512]{1,0:T(8,128)(2,1)S(1)}, u32[]{:S(2)}, u32[]{:S(2)}) collective-permute-start(bf16[64,512]{1,0:T(8,128)(2,1)} %get-tuple-element.26), channel_id=1, source_target_pairs={{0,8},{8,16},{16,24},{24,32},{32,40},{40,48},{48,56},{56,64},{64,7... | collective-permute-start | bytes 196616 | tf_op jit(solution)/shard_map/ppermute | solution.py:422
  13.5 4.3 %all-to-all-start = ((bf16[4,256,512]{2,1,0:T(8,128)(2,1)}), bf16[4,256,512]{2,1,0:T(8,128)(2,1)}, u32[]{:S(2)}, u32[]{:S(2)}) async-start(bf16[4,256,512]{2,1,0:T(8,128)(2,1)} %get-tuple-element.29), calls=%async_computation | async-start | bytes 2097152 | tf_op jit(solution)/shard_map/all_to_all | solution.py:434
  17.8 0.0 collective-permute-done.halo_ref.halo_hbm
  17.8 0.0 copy-start.5
  17.8 0.0 copy-done.3
  17.8 0.0 copy-done.2
  17.8 0.0 copy-done.4
  17.8 0.0 copy-done.7
  17.8 0.0 copy-done.6
  17.9 0.0 copy-start.1
  17.9 4.8 %module_forward.1 = (bf16[512,512]{1,0:T(8,128)(2,1)S(1)}, f32[4,512,128]{2,1,0:T(8,128)}, f32[512,128]{1,0:T(8,128)}) custom-call(f32[31,512]{1,0:T(8,128)S(1)} %copy-done.4, f32[1,512]{1,0:T(1,128)S(1)} %bitcast.21, f32[1,512]{1,0:T(1,128)S(1)} %bitcast.23, bf16[64,512]{1,0:T(8,128)(2,1)S(1)} %collective-permute-done.halo_ref.halo_hbm, ...), custom_call_target="tpu_custom_call" | custom-call | flops 3000000000 | bytes 1048576 | tf_op jit(solution)/shard_map/module_forward/pallas_call | solution.py:466
  22.6 0.0 copy-done.5
  22.6 1.9 %collective-permute-start.1 = (bf16[512,512]{1,0:T(8,128)(2,1)S(1)}, bf16[512,512]{1,0:T(8,128)(2,1)S(1)}, u32[]{:S(2)}, u32[]{:S(2)}) collective-permute-start(bf16[512,512]{1,0:T(8,128)(2,1)S(1)} %get-tuple-element.30.act_ref), channel_id=1, source_target_pairs={{0,1},{1,0},{2,3},{3,2},{4,5},{5,4},{6,7},{7,6},{8,9},{9,8},{10,11... | collective-permute-start | bytes 1572872 | tf_op jit(solution)/shard_map/ppermute | solution.py:426
  24.6 1.9 %collective-permute-done.1.other_act_ref = bf16[512,512]{1,0:T(8,128)(2,1)S(1)} collective-permute-done((bf16[512,512]{1,0:T(8,128)(2,1)S(1)}, bf16[512,512]{1,0:T(8,128)(2,1)S(1)}, u32[]{:S(2)}, u32[]{:S(2)}) %collective-permute-start.1) | collective-permute-done | bytes 524320 | tf_op jit(solution)/shard_map/ppermute | solution.py:426
  26.4 0.0 collective-permute-done.2.other_cotan_ref
  26.5 0.0 copy-done.1
  26.5 3.7 %weight_term.1 = (bf16[4,256,512]{2,1,0:T(8,128)(2,1)}, f32[256,512]{1,0:T(8,128)}) custom-call(bf16[512,512]{1,0:T(8,128)(2,1)S(1)} %get-tuple-element.30.act_ref, bf16[512,512]{1,0:T(8,128)(2,1)S(1)} %collective-permute-done.1.other_act_ref, bf16[512,2048]{1,0:T(8,128)(2,1)S(1)} %bitcast.11, bf16[512,2048]{1,0:T(8,128)(2,1)} %collective-permute-done.2.other_cotan_ref), custom_call_target="tpu_custom_call" | custom-call | flops 1500000000 | bytes 1048576 | tf_op jit(solution)/shard_map/weight_term/pallas_call | solution.py:486
  30.2 2.9 %all-to-all-done.own_hbm = bf16[4,256,512]{2,1,0:T(8,128)(2,1)} async-done(((bf16[4,256,512]{2,1,0:T(8,128)(2,1)}), bf16[4,256,512]{2,1,0:T(8,128)(2,1)}, u32[]{:S(2)}, u32[]{:S(2)}) %all-to-all-start) | async-done | bytes 1048608 | tf_op jit(solution)/shard_map/all_to_all | solution.py:434
  33.0 2.8 %collective-permute-start.3 = (bf16[4,256,512]{2,1,0:T(8,128)(2,1)}, bf16[4,256,512]{2,1,0:T(8,128)(2,1)S(1)}, u32[]{:S(2)}, u32[]{:S(2)}) collective-permute-start(bf16[4,256,512]{2,1,0:T(8,128)(2,1)} %all-to-all-done.own_hbm), channel_id=1, source_target_pairs={{0,1},{1,0},{2,3},{3,2},{4,5},{5,4},{6,7},{7,6},{8,9},{9,8},{10,11... | collective-permute-start | bytes 3145736 | tf_op jit(solution)/shard_map/ppermute | solution.py:426
  35.8 3.5 %all-to-all-start.1 = ((bf16[4,256,512]{2,1,0:T(8,128)(2,1)}), bf16[4,256,512]{2,1,0:T(8,128)(2,1)S(1)}, u32[]{:S(2)}, u32[]{:S(2)}) async-start(bf16[4,256,512]{2,1,0:T(8,128)(2,1)} %get-tuple-element.37), calls=%async_computation.1 | async-start | bytes 2097152 | tf_op jit(solution)/shard_map/all_to_all | solution.py:434
  39.3 0.0 collective-permute-done.3.other_ref
  39.3 0.0 copy-start
  39.4 7.1 %module_backward.1 = (f32[4,512,128]{2,1,0:T(8,128)}, f32[4,32,128]{2,1,0:T(8,128)S(1)}, f32[4,40,128]{2,1,0:T(8,128)S(1)}) custom-call(f32[1,512]{1,0:T(1,128)} %bitcast.20, f32[1,512]{1,0:T(1,128)} %bitcast.22, f32[4,512,128]{2,1,0:T(8,128)} %get-tuple-element.27.normed_hbm, f32[512,128]{1,0:T(8,128)} %get-tuple-element.28.inv_hbm, ...), custom_call_target="tpu_custom_call" | custom-call | flops 5000000000 | bytes 1048576 | tf_op jit(solution)/shard_map/module_backward/pallas_call | solution.py:505
  46.5 8.0 %all-to-all-done.1.parts_ref = bf16[4,256,512]{2,1,0:T(8,128)(2,1)S(1)} async-done(((bf16[4,256,512]{2,1,0:T(8,128)(2,1)}), bf16[4,256,512]{2,1,0:T(8,128)(2,1)S(1)}, u32[]{:S(2)}, u32[]{:S(2)}) %all-to-all-start.1) | async-done | bytes 1048608 | tf_op jit(solution)/shard_map/all_to_all | solution.py:434
  54.5 0.0 copy-done
  54.5 0.3 pack.1
  54.7 26.5 %all_to_all.25.parts_ref = bf16[64,24,128]{2,1,0:T(8,128)(2,1)S(1)} all-to-all(bf16[64,24,128]{2,1,0:T(8,128)(2,1)S(1)} %pack.1), channel_id=1, replica_groups=mesh['sp_0'=8,'sp_1'=8,'dp_0'=4,'dp_1'=2] {'sp_0','sp_1'}, dimensions={0} | all-to-all | bytes 786432 | tf_op jit(solution)/shard_map/all_to_all | solution.py:434
  81.2 0.1 total.1
  81.3 10.7 %all_to_all.26.tiles_ref = f32[8,8,128]{2,1,0:T(8,128)S(1)} all-to-all(f32[8,8,128]{2,1,0:T(8,128)S(1)} %get-tuple-element.41), channel_id=1, replica_groups=mesh['sp_0'=8,'sp_1'=8,'dp_0'=4,'dp_1'=2] {'dp_0','dp_1'}, dimensions={0} | all-to-all | bytes 65536 | tf_op jit(solution)/shard_map/all_to_all | solution.py:434
  92.0 0.8 spread.1
  92.8 4.6 %all-to-all-start.4 = ((bf16[64,24,128]{2,1,0:T(8,128)(2,1)}), bf16[64,24,128]{2,1,0:T(8,128)(2,1)S(1)}, u32[]{:S(2)}, u32[]{:S(2)}) async-start(bf16[64,24,128]{2,1,0:T(8,128)(2,1)} %spread.1), calls=%async_computation.4 | async-start | bytes 786432 | tf_op jit(solution)/shard_map/all_to_all | solution.py:434
  97.4 1.3 %collective-permute-start.4 = (f32[4,32,128]{2,1,0:T(8,128)S(1)}, f32[4,32,128]{2,1,0:T(8,128)S(1)}, u32[]{:S(2)}, u32[]{:S(2)}) collective-permute-start(f32[4,32,128]{2,1,0:T(8,128)S(1)} %get-tuple-element.33), channel_id=1, source_target_pairs={{8,0},{16,8},{24,16},{32,24},{40,32},{48,40},{56,48},{64,56},{72,6... | collective-permute-start | bytes 196616 | tf_op jit(solution)/shard_map/ppermute | solution.py:422
  98.7 9.0 %collective-permute-done.4.later_ref = f32[4,32,128]{2,1,0:T(8,128)S(1)} collective-permute-done((f32[4,32,128]{2,1,0:T(8,128)S(1)}, f32[4,32,128]{2,1,0:T(8,128)S(1)}, u32[]{:S(2)}, u32[]{:S(2)}) %collective-permute-start.4) | collective-permute-done | bytes 65568 | tf_op jit(solution)/shard_map/ppermute | solution.py:422
  107.7 0.0 copy-start.8
  107.7 0.6 copy-done.8
  108.3 6.0 %gated_backward.1 = (bf16[512,512]{1,0:T(8,128)(2,1)}, bf16[512,512]{1,0:T(8,128)(2,1)}) custom-call(f32[4,32,128]{2,1,0:T(8,128)} %copy-done.8, f32[31,512]{1,0:T(8,128)} %taps_ref.3, f32[4,512,128]{2,1,0:T(8,128)} %get-tuple-element.34.grad_hbm, bf16[512,512]{1,0:T(8,128)(2,1)} %bitcast.14, bf16[512,512]{1,0:T(8,128)(2,1)} %bitcast.18), custom_call_target="tpu_custom_call" | custom-call | flops 3000000000 | bytes 1048576 | tf_op jit(solution)/shard_map/gated_backward/pallas_call | solution.py:548
  114.4 0.0 all-to-all-done.4.parts_ref
  114.4 0.9 unpack.1
Async XLA Ops:
  0.6 17.2 %copy-start.3 = (bf16[1,512,512]{2,1,0:T(8,128)(2,1)S(1)}, bf16[1,512,512]{2,1,0:T(8,128)(2,1)}, u32[]{:S(2)}) copy-start(bf16[1,512,512]{2,1,0:T(8,128)(2,1)} %param.8) | copy-start | bytes 1572868
  0.6 17.2 %copy-start.2 = (bf16[1,512,512]{2,1,0:T(8,128)(2,1)S(1)}, bf16[1,512,512]{2,1,0:T(8,128)(2,1)}, u32[]{:S(2)}) copy-start(bf16[1,512,512]{2,1,0:T(8,128)(2,1)} %param.7) | copy-start | bytes 1572868
  0.7 17.2 %copy-start.4 = (f32[31,512]{1,0:T(8,128)S(1)}, f32[31,512]{1,0:T(8,128)}, u32[]{:S(2)}) copy-start(f32[31,512]{1,0:T(8,128)} %taps_ref.3) | copy-start | bytes 190468
  0.7 17.2 %copy-start.7 = (f32[512]{0:T(512)S(1)}, f32[512]{0:T(512)}, u32[]{:S(2)}) copy-start(f32[512]{0:T(512)} %param.12) | copy-start | bytes 6148
  0.7 17.2 %copy-start.6 = (f32[512]{0:T(512)S(1)}, f32[512]{0:T(512)}, u32[]{:S(2)}) copy-start(f32[512]{0:T(512)} %param.11) | copy-start | bytes 6148
  0.7 25.8 %collective-permute-start.2 = (bf16[512,2048]{1,0:T(8,128)(2,1)}, bf16[512,2048]{1,0:T(8,128)(2,1)}, u32[]{:S(2)}, u32[]{:S(2)}) collective-permute-start(bf16[512,2048]{1,0:T(8,128)(2,1)} %bitcast.9), channel_id=1, source_target_pairs={{0,1},{1,0},{2,3},{3,2},{4,5},{5,4},{6,7},{7,6},{8,9},{9,8},{10,11... | collective-permute-start | bytes 6291464 | tf_op jit(solution)/shard_map/ppermute | solution.py:426
  12.2 5.6 %collective-permute-start = (bf16[64,512]{1,0:T(8,128)(2,1)}, bf16[64,512]{1,0:T(8,128)(2,1)S(1)}, u32[]{:S(2)}, u32[]{:S(2)}) collective-permute-start(bf16[64,512]{1,0:T(8,128)(2,1)} %get-tuple-element.26), channel_id=1, source_target_pairs={{0,8},{8,16},{16,24},{24,32},{32,40},{40,48},{48,56},{56,64},{64,7... | collective-permute-start | bytes 196616 | tf_op jit(solution)/shard_map/ppermute | solution.py:422
  13.5 19.5 %all-to-all-start = ((bf16[4,256,512]{2,1,0:T(8,128)(2,1)}), bf16[4,256,512]{2,1,0:T(8,128)(2,1)}, u32[]{:S(2)}, u32[]{:S(2)}) async-start(bf16[4,256,512]{2,1,0:T(8,128)(2,1)} %get-tuple-element.29), calls=%async_computation | async-start | bytes 2097152 | tf_op jit(solution)/shard_map/all_to_all | solution.py:434
  17.8 4.8 %copy-start.5 = (bf16[64,512]{1,0:T(8,128)(2,1)}, bf16[64,512]{1,0:T(8,128)(2,1)S(1)}, u32[]{:S(2)}) copy-start(bf16[64,512]{1,0:T(8,128)(2,1)S(1)} %collective-permute-done.halo_ref.halo_hbm) | copy-start | bytes 196612
  17.9 8.6 %copy-start.1 = (bf16[1,512,2048]{2,1,0:T(8,128)(2,1)S(1)}, bf16[1,512,2048]{2,1,0:T(8,128)(2,1)}, u32[]{:S(2)}) copy-start(bf16[1,512,2048]{2,1,0:T(8,128)(2,1)} %param.9) | copy-start | bytes 6291460
  22.6 3.8 %collective-permute-start.1 = (bf16[512,512]{1,0:T(8,128)(2,1)S(1)}, bf16[512,512]{1,0:T(8,128)(2,1)S(1)}, u32[]{:S(2)}, u32[]{:S(2)}) collective-permute-start(bf16[512,512]{1,0:T(8,128)(2,1)S(1)} %get-tuple-element.30.act_ref), channel_id=1, source_target_pairs={{0,1},{1,0},{2,3},{3,2},{4,5},{5,4},{6,7},{7,6},{8,9},{9,8},{10,11... | collective-permute-start | bytes 1572872 | tf_op jit(solution)/shard_map/ppermute | solution.py:426
  33.0 6.3 %collective-permute-start.3 = (bf16[4,256,512]{2,1,0:T(8,128)(2,1)}, bf16[4,256,512]{2,1,0:T(8,128)(2,1)S(1)}, u32[]{:S(2)}, u32[]{:S(2)}) collective-permute-start(bf16[4,256,512]{2,1,0:T(8,128)(2,1)} %all-to-all-done.own_hbm), channel_id=1, source_target_pairs={{0,1},{1,0},{2,3},{3,2},{4,5},{5,4},{6,7},{7,6},{8,9},{9,8},{10,11... | collective-permute-start | bytes 3145736 | tf_op jit(solution)/shard_map/ppermute | solution.py:426
  35.8 18.7 %all-to-all-start.1 = ((bf16[4,256,512]{2,1,0:T(8,128)(2,1)}), bf16[4,256,512]{2,1,0:T(8,128)(2,1)S(1)}, u32[]{:S(2)}, u32[]{:S(2)}) async-start(bf16[4,256,512]{2,1,0:T(8,128)(2,1)} %get-tuple-element.37), calls=%async_computation.1 | async-start | bytes 2097152 | tf_op jit(solution)/shard_map/all_to_all | solution.py:434
  39.3 15.1 %copy-start = (f32[256,512]{1,0:T(8,128)S(1)}, f32[256,512]{1,0:T(8,128)}, u32[]{:S(2)}) copy-start(f32[256,512]{1,0:T(8,128)} %get-tuple-element.38.kept_ref) | copy-start | bytes 1572868
  92.8 21.6 %all-to-all-start.4 = ((bf16[64,24,128]{2,1,0:T(8,128)(2,1)}), bf16[64,24,128]{2,1,0:T(8,128)(2,1)S(1)}, u32[]{:S(2)}, u32[]{:S(2)}) async-start(bf16[64,24,128]{2,1,0:T(8,128)(2,1)} %spread.1), calls=%async_computation.4 | async-start | bytes 786432 | tf_op jit(solution)/shard_map/all_to_all | solution.py:434
  97.4 10.3 %collective-permute-start.4 = (f32[4,32,128]{2,1,0:T(8,128)S(1)}, f32[4,32,128]{2,1,0:T(8,128)S(1)}, u32[]{:S(2)}, u32[]{:S(2)}) collective-permute-start(f32[4,32,128]{2,1,0:T(8,128)S(1)} %get-tuple-element.33), channel_id=1, source_target_pairs={{8,0},{16,8},{24,16},{32,24},{40,32},{48,40},{56,48},{64,56},{72,6... | collective-permute-start | bytes 196616 | tf_op jit(solution)/shard_map/ppermute | solution.py:422
  107.7 0.6 copy-start.8

commit v4 on v3

--- a/solution.py
+++ b/solution.py
@@ -378,13 +378,13 @@
         0, parts_ref.shape[0], add, jnp.zeros(parts_ref.shape[1:], F32), unroll=8
     ) * scale
     rows_ref[...] = total[0:16]
-    tile = jnp.concatenate([total[16:20] + total[20:24], jnp.zeros((4, LANES), F32)], axis=0)
+    tile = total[16:20] + total[20:24]
     for i in range(tiles_ref.shape[0]):
         tiles_ref[i] = tile
 
 
 def spread_kernel(rows_ref, tiles_ref, out_ref):
-    tile = sum(tiles_ref[i] for i in range(tiles_ref.shape[0]))[0:4]
+    tile = sum(tiles_ref[i] for i in range(tiles_ref.shape[0]))
     high = tile.astype(BF16).astype(F32)
     both = jnp.concatenate([rows_ref[...], high, tile - high], axis=0).astype(BF16)
 
@@ -395,12 +395,16 @@
     lax.fori_loop(0, out_ref.shape[0], put, 0, unroll=8)
 
 
-def unpack_kernel(parts_ref, weight_ref, taps_ref, gain_ref, shift_ref, small_ref):
+def unpack_kernel(
+    parts_ref, weight_hbm, taps_ref, gain_ref, shift_ref, small_ref, weight_ref, sems
+):
     count = parts_ref.shape[0]
     small_rows = small_ref.shape[0]
     tap_count = taps_ref.shape[0]
     blocks = small_ref.shape[1] // LANES
     halves = small_rows // 4
+    rows = weight_ref.shape[0] // 4
+    stores = []
     for m in range(count):
         i, h = m // 2, m % 2
         part = parts_ref[m].astype(F32)
@@ -411,9 +415,18 @@
         if m < blocks * halves:
             b, g = m // halves, m % halves
             small_ref[4 * g : 4 * g + 4, b * LANES : (b + 1) * LANES] = part[16:20] + part[20:24]
+        if (m + 1) % (count // 4) == 0:
+            n = m // (count // 4)
+            span = pl.ds(n * rows, rows)
+            stores.append(
+                pltpu.make_async_copy(weight_ref.at[span], weight_hbm.at[span], sems.at[n])
+            )
+            stores[-1].start()
     taps_ref[...] = small_ref[0:tap_count, :]
     gain_ref[...] = small_ref[tap_count : tap_count + 1, :]
     shift_ref[...] = small_ref[tap_count + 1 : tap_count + 2, :]
+    for store in stores:
+        store.wait()
 
 
 def from_behind(value, axis, by):
@@ -564,7 +577,7 @@
     terms = exchanged(packed, SP)
     rows, tiles = pl.pallas_call(
         functools.partial(total_kernel, scale),
-        out_shape=(shaped((16, LANES), F32), shaped((count_dp, 8, LANES), F32)),
+        out_shape=(shaped((16, LANES), F32), shaped((count_dp, 4, LANES), F32)),
         in_specs=[VMEM],
         out_specs=(VMEM,) * 2,
         compiler_params=params(4),
@@ -591,8 +604,12 @@
             shaped((1, channels), F32),
         ),
         in_specs=[VMEM],
-        out_specs=(VMEM,) * 4,
-        scratch_shapes=[pltpu.VMEM((small_rows, channels), F32)],
+        out_specs=(HBM,) + (VMEM,) * 3,
+        scratch_shapes=[
+            pltpu.VMEM((small_rows, channels), F32),
+            pltpu.VMEM((wide, channels), F32),
+            pltpu.SemaphoreType.DMA((4,)),
+        ],
         compiler_params=params(8),
         cost_estimate=cost(1),
         name="unpack",

time: 117 us -> 118 us (level)
  no operation moved by 1% of the time
where the time goes in v4:
time: 118 us; the launch traced here: 116 us
  blocking collectives  37.1 us (31%)
  starting transfers between devices  28.6 us (24%)
  Pallas kernels  26.8 us (23%)
  waiting for transfers between devices  21.7 us (18%)
    all_to_all x2, blocking collectives, exchanged(): return lax.all_to_all(value, axes, 0, 0, tiled=True)  37.1 us
    ppermute x3, starting transfers between devices, swapped(): return lax.ppermute(value, 'dp_1', [(0, 1), (1, 0)])  13.6 us
    all_to_all x3, starting transfers between devices, exchanged(): return lax.all_to_all(value, axes, 0, 0, tiled=True)  12.4 us
    all_to_all x3, waiting for transfers between devices, exchanged(): return lax.all_to_all(value, axes, 0, 0, tiled=True)  10.8 us
    ppermute x2, waiting for transfers between devices, from_behind(): return lax.ppermute(value, axis, pairs)  8.98 us
    pallas_call x1, Pallas kernels, one_device(): pl.pallas_call(backward_kernel, out_shape=(pltpu.HBM((blocks, length, LAN...  7.13 us
    pallas_call x1, Pallas kernels, one_device(): pl.pallas_call(gated_kernel, out_shape=(shaped((length, channels), BF16),...  6 us
    pallas_call x1, Pallas kernels, one_device(): pl.pallas_call(forward_kernel, out_shape=(shaped((length, channels), BF16...  4.76 us
  transfers between devices with their start and end apart: 8, of which 4 were waited for; matrix products, arithmetic and copies ran while one was open for 0% of the time, Pallas kernels for 21%

profile of v4, /device:TPU:1, one launch (start us, length us, event | category | flops | bytes accessed | tf_op | source)
XLA Modules:
  0.0 115.8 jit_solution(3132191249043971290)
XLA Ops:
  0.6 0.0 copy-start.3
  0.6 0.0 copy-start.2
  0.7 0.0 copy-start.4
  0.7 0.0 copy-start.7
  0.7 0.0 copy-start.6
  0.7 8.9 %collective-permute-start.2 = (bf16[512,2048]{1,0:T(8,128)(2,1)}, bf16[512,2048]{1,0:T(8,128)(2,1)}, u32[]{:S(2)}, u32[]{:S(2)}) collective-permute-start(bf16[512,2048]{1,0:T(8,128)(2,1)} %bitcast.9), channel_id=1, source_target_pairs={{0,1},{1,0},{2,3},{3,2},{4,5},{5,4},{6,7},{7,6},{8,9},{9,8},{10,11... | collective-permute-start | bytes 6291464 | tf_op jit(solution)/shard_map/ppermute | solution.py:439
  9.6 2.6 %prepare.1 = (bf16[64,512]{1,0:T(8,128)(2,1)}, bf16[4,256,512]{2,1,0:T(8,128)(2,1)}) custom-call(bf16[512,512]{1,0:T(8,128)(2,1)} %bitcast.12, bf16[512,512]{1,0:T(8,128)(2,1)} %bitcast.16, bf16[256,512]{1,0:T(8,128)(2,1)} %weight_hbm.1), custom_call_target="tpu_custom_call" | custom-call | flops 500000000 | bytes 1048576 | tf_op jit(solution)/shard_map/prepare/pallas_call | solution.py:465
  12.2 1.3 %collective-permute-start = (bf16[64,512]{1,0:T(8,128)(2,1)}, bf16[64,512]{1,0:T(8,128)(2,1)S(1)}, u32[]{:S(2)}, u32[]{:S(2)}) collective-permute-start(bf16[64,512]{1,0:T(8,128)(2,1)} %get-tuple-element.26), channel_id=1, source_target_pairs={{0,8},{8,16},{16,24},{24,32},{32,40},{40,48},{48,56},{56,64},{64,7... | collective-permute-start | bytes 196616 | tf_op jit(solution)/shard_map/ppermute | solution.py:435
  13.5 4.3 %all-to-all-start = ((bf16[4,256,512]{2,1,0:T(8,128)(2,1)}), bf16[4,256,512]{2,1,0:T(8,128)(2,1)}, u32[]{:S(2)}, u32[]{:S(2)}) async-start(bf16[4,256,512]{2,1,0:T(8,128)(2,1)} %get-tuple-element.29), calls=%async_computation | async-start | bytes 2097152 | tf_op jit(solution)/shard_map/all_to_all | solution.py:447
  17.8 0.0 collective-permute-done.halo_ref.halo_hbm
  17.8 0.0 copy-start.5
  17.8 0.0 copy-done.3
  17.8 0.0 copy-done.2
  17.8 0.0 copy-done.4
  17.8 0.0 copy-done.7
  17.8 0.0 copy-done.6
  17.9 0.0 copy-start.1
  17.9 4.8 %module_forward.1 = (bf16[512,512]{1,0:T(8,128)(2,1)S(1)}, f32[4,512,128]{2,1,0:T(8,128)}, f32[512,128]{1,0:T(8,128)}) custom-call(f32[31,512]{1,0:T(8,128)S(1)} %copy-done.4, f32[1,512]{1,0:T(1,128)S(1)} %bitcast.21, f32[1,512]{1,0:T(1,128)S(1)} %bitcast.23, bf16[64,512]{1,0:T(8,128)(2,1)S(1)} %collective-permute-done.halo_ref.halo_hbm, ...), custom_call_target="tpu_custom_call" | custom-call | flops 3000000000 | bytes 1048576 | tf_op jit(solution)/shard_map/module_forward/pallas_call | solution.py:479
  22.6 0.0 copy-done.5
  22.6 1.9 %collective-permute-start.1 = (bf16[512,512]{1,0:T(8,128)(2,1)S(1)}, bf16[512,512]{1,0:T(8,128)(2,1)S(1)}, u32[]{:S(2)}, u32[]{:S(2)}) collective-permute-start(bf16[512,512]{1,0:T(8,128)(2,1)S(1)} %get-tuple-element.30.act_ref), channel_id=1, source_target_pairs={{0,1},{1,0},{2,3},{3,2},{4,5},{5,4},{6,7},{7,6},{8,9},{9,8},{10,11... | collective-permute-start | bytes 1572872 | tf_op jit(solution)/shard_map/ppermute | solution.py:439
  24.6 1.9 %collective-permute-done.1.other_act_ref = bf16[512,512]{1,0:T(8,128)(2,1)S(1)} collective-permute-done((bf16[512,512]{1,0:T(8,128)(2,1)S(1)}, bf16[512,512]{1,0:T(8,128)(2,1)S(1)}, u32[]{:S(2)}, u32[]{:S(2)}) %collective-permute-start.1) | collective-permute-done | bytes 524320 | tf_op jit(solution)/shard_map/ppermute | solution.py:439
  26.4 0.0 collective-permute-done.2.other_cotan_ref
  26.5 0.0 copy-done.1
  26.5 3.7 %weight_term.1 = (bf16[4,256,512]{2,1,0:T(8,128)(2,1)}, f32[256,512]{1,0:T(8,128)}) custom-call(bf16[512,512]{1,0:T(8,128)(2,1)S(1)} %get-tuple-element.30.act_ref, bf16[512,512]{1,0:T(8,128)(2,1)S(1)} %collective-permute-done.1.other_act_ref, bf16[512,2048]{1,0:T(8,128)(2,1)S(1)} %bitcast.11, bf16[512,2048]{1,0:T(8,128)(2,1)} %collective-permute-done.2.other_cotan_ref), custom_call_target="tpu_custom_call" | custom-call | flops 1500000000 | bytes 1048576 | tf_op jit(solution)/shard_map/weight_term/pallas_call | solution.py:499
  30.2 2.9 %all-to-all-done.own_hbm = bf16[4,256,512]{2,1,0:T(8,128)(2,1)} async-done(((bf16[4,256,512]{2,1,0:T(8,128)(2,1)}), bf16[4,256,512]{2,1,0:T(8,128)(2,1)}, u32[]{:S(2)}, u32[]{:S(2)}) %all-to-all-start) | async-done | bytes 1048608 | tf_op jit(solution)/shard_map/all_to_all | solution.py:447
  33.0 2.8 %collective-permute-start.3 = (bf16[4,256,512]{2,1,0:T(8,128)(2,1)}, bf16[4,256,512]{2,1,0:T(8,128)(2,1)S(1)}, u32[]{:S(2)}, u32[]{:S(2)}) collective-permute-start(bf16[4,256,512]{2,1,0:T(8,128)(2,1)} %all-to-all-done.own_hbm), channel_id=1, source_target_pairs={{0,1},{1,0},{2,3},{3,2},{4,5},{5,4},{6,7},{7,6},{8,9},{9,8},{10,11... | collective-permute-start | bytes 3145736 | tf_op jit(solution)/shard_map/ppermute | solution.py:439
  35.8 3.5 %all-to-all-start.1 = ((bf16[4,256,512]{2,1,0:T(8,128)(2,1)}), bf16[4,256,512]{2,1,0:T(8,128)(2,1)S(1)}, u32[]{:S(2)}, u32[]{:S(2)}) async-start(bf16[4,256,512]{2,1,0:T(8,128)(2,1)} %get-tuple-element.37), calls=%async_computation.1 | async-start | bytes 2097152 | tf_op jit(solution)/shard_map/all_to_all | solution.py:447
  39.3 0.0 collective-permute-done.3.other_ref
  39.3 0.0 copy-start
  39.4 7.1 %module_backward.1 = (f32[4,512,128]{2,1,0:T(8,128)}, f32[4,32,128]{2,1,0:T(8,128)S(1)}, f32[4,40,128]{2,1,0:T(8,128)S(1)}) custom-call(f32[1,512]{1,0:T(1,128)} %bitcast.20, f32[1,512]{1,0:T(1,128)} %bitcast.22, f32[4,512,128]{2,1,0:T(8,128)} %get-tuple-element.27.normed_hbm, f32[512,128]{1,0:T(8,128)} %get-tuple-element.28.inv_hbm, ...), custom_call_target="tpu_custom_call" | custom-call | flops 5000000000 | bytes 1048576 | tf_op jit(solution)/shard_map/module_backward/pallas_call | solution.py:518
  46.5 8.0 %all-to-all-done.1.parts_ref = bf16[4,256,512]{2,1,0:T(8,128)(2,1)S(1)} async-done(((bf16[4,256,512]{2,1,0:T(8,128)(2,1)}), bf16[4,256,512]{2,1,0:T(8,128)(2,1)S(1)}, u32[]{:S(2)}, u32[]{:S(2)}) %all-to-all-start.1) | async-done | bytes 1048608 | tf_op jit(solution)/shard_map/all_to_all | solution.py:447
  54.5 0.0 copy-done
  54.5 0.3 pack.1
  54.7 26.5 %all_to_all.25.parts_ref = bf16[64,24,128]{2,1,0:T(8,128)(2,1)S(1)} all-to-all(bf16[64,24,128]{2,1,0:T(8,128)(2,1)S(1)} %pack.1), channel_id=1, replica_groups=mesh['sp_0'=8,'sp_1'=8,'dp_0'=4,'dp_1'=2] {'sp_0','sp_1'}, dimensions={0} | all-to-all | bytes 786432 | tf_op jit(solution)/shard_map/all_to_all | solution.py:447
  81.2 0.1 total.1
  81.3 10.6 %all_to_all.26.tiles_ref = f32[8,4,128]{2,1,0:T(4,128)S(1)} all-to-all(f32[8,4,128]{2,1,0:T(4,128)S(1)} %get-tuple-element.41), channel_id=1, replica_groups=mesh['sp_0'=8,'sp_1'=8,'dp_0'=4,'dp_1'=2] {'dp_0','dp_1'}, dimensions={0} | all-to-all | bytes 32768 | tf_op jit(solution)/shard_map/all_to_all | solution.py:447
  91.9 0.8 spread.1
  92.7 4.6 %all-to-all-start.4 = ((bf16[64,24,128]{2,1,0:T(8,128)(2,1)}), bf16[64,24,128]{2,1,0:T(8,128)(2,1)S(1)}, u32[]{:S(2)}, u32[]{:S(2)}) async-start(bf16[64,24,128]{2,1,0:T(8,128)(2,1)} %spread.1), calls=%async_computation.4 | async-start | bytes 786432 | tf_op jit(solution)/shard_map/all_to_all | solution.py:447
  97.4 1.3 %collective-permute-start.4 = (f32[4,32,128]{2,1,0:T(8,128)S(1)}, f32[4,32,128]{2,1,0:T(8,128)S(1)}, u32[]{:S(2)}, u32[]{:S(2)}) collective-permute-start(f32[4,32,128]{2,1,0:T(8,128)S(1)} %get-tuple-element.33), channel_id=1, source_target_pairs={{8,0},{16,8},{24,16},{32,24},{40,32},{48,40},{56,48},{64,56},{72,6... | collective-permute-start | bytes 196616 | tf_op jit(solution)/shard_map/ppermute | solution.py:435
  98.7 9.0 %collective-permute-done.4.later_ref = f32[4,32,128]{2,1,0:T(8,128)S(1)} collective-permute-done((f32[4,32,128]{2,1,0:T(8,128)S(1)}, f32[4,32,128]{2,1,0:T(8,128)S(1)}, u32[]{:S(2)}, u32[]{:S(2)}) %collective-permute-start.4) | collective-permute-done | bytes 65568 | tf_op jit(solution)/shard_map/ppermute | solution.py:435
  107.6 0.0 copy-start.8
  107.6 0.6 copy-done.8
  108.3 6.0 %gated_backward.1 = (bf16[512,512]{1,0:T(8,128)(2,1)}, bf16[512,512]{1,0:T(8,128)(2,1)}) custom-call(f32[4,32,128]{2,1,0:T(8,128)} %copy-done.8, f32[31,512]{1,0:T(8,128)} %taps_ref.3, f32[4,512,128]{2,1,0:T(8,128)} %get-tuple-element.34.grad_hbm, bf16[512,512]{1,0:T(8,128)(2,1)} %bitcast.14, bf16[512,512]{1,0:T(8,128)(2,1)} %bitcast.18), custom_call_target="tpu_custom_call" | custom-call | flops 3000000000 | bytes 1048576 | tf_op jit(solution)/shard_map/gated_backward/pallas_call | solution.py:561
  114.3 0.0 all-to-all-done.4.parts_ref
  114.3 1.5 %unpack.1 = (f32[256,512]{1,0:T(8,128)}, f32[31,512]{1,0:T(8,128)}, f32[1,512]{1,0:T(1,128)}, f32[1,512]{1,0:T(1,128)}) custom-call(bf16[64,24,128]{2,1,0:T(8,128)(2,1)S(1)} %all-to-all-done.4.parts_ref), custom_call_target="tpu_custom_call" | custom-call | flops 500000000 | bytes 1048576 | tf_op jit(solution)/shard_map/unpack/pallas_call | solution.py:598
Async XLA Ops:
  0.6 17.2 %copy-start.3 = (bf16[1,512,512]{2,1,0:T(8,128)(2,1)S(1)}, bf16[1,512,512]{2,1,0:T(8,128)(2,1)}, u32[]{:S(2)}) copy-start(bf16[1,512,512]{2,1,0:T(8,128)(2,1)} %param.8) | copy-start | bytes 1572868
  0.6 17.2 %copy-start.2 = (bf16[1,512,512]{2,1,0:T(8,128)(2,1)S(1)}, bf16[1,512,512]{2,1,0:T(8,128)(2,1)}, u32[]{:S(2)}) copy-start(bf16[1,512,512]{2,1,0:T(8,128)(2,1)} %param.7) | copy-start | bytes 1572868
  0.7 17.2 %copy-start.4 = (f32[31,512]{1,0:T(8,128)S(1)}, f32[31,512]{1,0:T(8,128)}, u32[]{:S(2)}) copy-start(f32[31,512]{1,0:T(8,128)} %taps_ref.3) | copy-start | bytes 190468
  0.7 17.2 %copy-start.7 = (f32[512]{0:T(512)S(1)}, f32[512]{0:T(512)}, u32[]{:S(2)}) copy-start(f32[512]{0:T(512)} %param.12) | copy-start | bytes 6148
  0.7 17.2 %copy-start.6 = (f32[512]{0:T(512)S(1)}, f32[512]{0:T(512)}, u32[]{:S(2)}) copy-start(f32[512]{0:T(512)} %param.11) | copy-start | bytes 6148
  0.7 25.8 %collective-permute-start.2 = (bf16[512,2048]{1,0:T(8,128)(2,1)}, bf16[512,2048]{1,0:T(8,128)(2,1)}, u32[]{:S(2)}, u32[]{:S(2)}) collective-permute-start(bf16[512,2048]{1,0:T(8,128)(2,1)} %bitcast.9), channel_id=1, source_target_pairs={{0,1},{1,0},{2,3},{3,2},{4,5},{5,4},{6,7},{7,6},{8,9},{9,8},{10,11... | collective-permute-start | bytes 6291464 | tf_op jit(solution)/shard_map/ppermute | solution.py:439
  12.2 5.6 %collective-permute-start = (bf16[64,512]{1,0:T(8,128)(2,1)}, bf16[64,512]{1,0:T(8,128)(2,1)S(1)}, u32[]{:S(2)}, u32[]{:S(2)}) collective-permute-start(bf16[64,512]{1,0:T(8,128)(2,1)} %get-tuple-element.26), channel_id=1, source_target_pairs={{0,8},{8,16},{16,24},{24,32},{32,40},{40,48},{48,56},{56,64},{64,7... | collective-permute-start | bytes 196616 | tf_op jit(solution)/shard_map/ppermute | solution.py:435
  13.5 19.5 %all-to-all-start = ((bf16[4,256,512]{2,1,0:T(8,128)(2,1)}), bf16[4,256,512]{2,1,0:T(8,128)(2,1)}, u32[]{:S(2)}, u32[]{:S(2)}) async-start(bf16[4,256,512]{2,1,0:T(8,128)(2,1)} %get-tuple-element.29), calls=%async_computation | async-start | bytes 2097152 | tf_op jit(solution)/shard_map/all_to_all | solution.py:447
  17.8 4.8 %copy-start.5 = (bf16[64,512]{1,0:T(8,128)(2,1)}, bf16[64,512]{1,0:T(8,128)(2,1)S(1)}, u32[]{:S(2)}) copy-start(bf16[64,512]{1,0:T(8,128)(2,1)S(1)} %collective-permute-done.halo_ref.halo_hbm) | copy-start | bytes 196612
  17.9 8.6 %copy-start.1 = (bf16[1,512,2048]{2,1,0:T(8,128)(2,1)S(1)}, bf16[1,512,2048]{2,1,0:T(8,128)(2,1)}, u32[]{:S(2)}) copy-start(bf16[1,512,2048]{2,1,0:T(8,128)(2,1)} %param.9) | copy-start | bytes 6291460
  22.6 3.8 %collective-permute-start.1 = (bf16[512,512]{1,0:T(8,128)(2,1)S(1)}, bf16[512,512]{1,0:T(8,128)(2,1)S(1)}, u32[]{:S(2)}, u32[]{:S(2)}) collective-permute-start(bf16[512,512]{1,0:T(8,128)(2,1)S(1)} %get-tuple-element.30.act_ref), channel_id=1, source_target_pairs={{0,1},{1,0},{2,3},{3,2},{4,5},{5,4},{6,7},{7,6},{8,9},{9,8},{10,11... | collective-permute-start | bytes 1572872 | tf_op jit(solution)/shard_map/ppermute | solution.py:439
  33.0 6.3 %collective-permute-start.3 = (bf16[4,256,512]{2,1,0:T(8,128)(2,1)}, bf16[4,256,512]{2,1,0:T(8,128)(2,1)S(1)}, u32[]{:S(2)}, u32[]{:S(2)}) collective-permute-start(bf16[4,256,512]{2,1,0:T(8,128)(2,1)} %all-to-all-done.own_hbm), channel_id=1, source_target_pairs={{0,1},{1,0},{2,3},{3,2},{4,5},{5,4},{6,7},{7,6},{8,9},{9,8},{10,11... | collective-permute-start | bytes 3145736 | tf_op jit(solution)/shard_map/ppermute | solution.py:439
  35.8 18.7 %all-to-all-start.1 = ((bf16[4,256,512]{2,1,0:T(8,128)(2,1)}), bf16[4,256,512]{2,1,0:T(8,128)(2,1)S(1)}, u32[]{:S(2)}, u32[]{:S(2)}) async-start(bf16[4,256,512]{2,1,0:T(8,128)(2,1)} %get-tuple-element.37), calls=%async_computation.1 | async-start | bytes 2097152 | tf_op jit(solution)/shard_map/all_to_all | solution.py:447
  39.3 15.1 %copy-start = (f32[256,512]{1,0:T(8,128)S(1)}, f32[256,512]{1,0:T(8,128)}, u32[]{:S(2)}) copy-start(f32[256,512]{1,0:T(8,128)} %get-tuple-element.38.kept_ref) | copy-start | bytes 1572868
  92.7 21.6 %all-to-all-start.4 = ((bf16[64,24,128]{2,1,0:T(8,128)(2,1)}), bf16[64,24,128]{2,1,0:T(8,128)(2,1)S(1)}, u32[]{:S(2)}, u32[]{:S(2)}) async-start(bf16[64,24,128]{2,1,0:T(8,128)(2,1)} %spread.1), calls=%async_computation.4 | async-start | bytes 786432 | tf_op jit(solution)/shard_map/all_to_all | solution.py:447
  97.4 10.3 %collective-permute-start.4 = (f32[4,32,128]{2,1,0:T(8,128)S(1)}, f32[4,32,128]{2,1,0:T(8,128)S(1)}, u32[]{:S(2)}, u32[]{:S(2)}) collective-permute-start(f32[4,32,128]{2,1,0:T(8,128)S(1)} %get-tuple-element.33), channel_id=1, source_target_pairs={{8,0},{16,8},{24,16},{32,24},{40,32},{48,40},{56,48},{64,56},{72,6... | collective-permute-start | bytes 196616 | tf_op jit(solution)/shard_map/ppermute | solution.py:435
  107.6 0.6 copy-start.8
